TPU v7x, 128 devices: a whole 4x4x4 slice. The times are simulated.
128 devices in a mesh: sp: 32 (over z, y, core), tp: 4 (over x).
Axes of the slice: x: 4, y: 4, z: 4, core: 2. Of those that a mesh axis runs over, the one named last changes fastest.
Arguments:
- tokens: bfloat16 [8192, 2048], P('sp'), may hold values from -6 to 6
- input_norm_gain: float32 [2048], replicated, may hold values from 0.1 to 1.9
- convolution_value_weight: bfloat16 [2048, 512], P(None, 'tp'), may hold values from -0.125 to 0.125
- convolution_gate_weight: bfloat16 [2048, 512], P(None, 'tp'), may hold values from -0.125 to 0.125
- depthwise_taps_weight: float32 [31, 512], P(None, 'tp'), may hold values from -1 to 1
- convolution_group_gain: float32 [512], P('tp'), may hold values from 0.1 to 1.9
- convolution_group_shift: float32 [512], P('tp'), may hold values from -3 to 3
- receptance_weight: bfloat16 [2048, 1024], P(None, 'tp'), may hold values from -0.125 to 0.125
- key_weight: bfloat16 [2048, 1024], P(None, 'tp'), may hold values from -0.125 to 0.125
- value_weight: bfloat16 [2048, 1024], P(None, 'tp'), may hold values from -0.125 to 0.125
- decay_weight: bfloat16 [2048, 1024], P(None, 'tp'), may hold values from -0.0625 to 0.0625
- correction_rate_weight: bfloat16 [2048, 1024], P(None, 'tp'), may hold values from -0.125 to 0.125
- output_gate_weight: bfloat16 [2048, 1024], P(None, 'tp'), may hold values from -0.125 to 0.125
- key_prenorm_gain: float32 [1024], P('tp'), may hold values from 0.04 to 8
- decay_offset_bias: float32 [1024], P('tp'), may hold values from -30 to 0
- position_decay_shift: float32 [8192, 1024], P('sp', 'tp'), may hold values from -1 to 1
- extra_log_decay: float32 [8192, 1024], P('sp', 'tp'), may hold values from -0.7 to 0
- head_norm_gain: float32 [1024], P('tp'), may hold values from 0.1 to 1.9
- convolution_output_weight: bfloat16 [512, 2048], replicated, may hold values from -0.15625 to 0.15625
- attention_output_weight: bfloat16 [1024, 2048], replicated, may hold values from -0.15625 to 0.15625
Outputs:
- mixed: bfloat16 [8192, 2048], P(('sp', 'tp'))
All inputs are finite; a program needn't handle non-finite values.
Results may differ from a plain program's by a relative error of at most 0.0063.
The roundings to bfloat16 on the way count: a program that leaves them out, or rounds other values in their place, can miss the bound.
Values may be sent and summed in bfloat16 or wider, within the bound.
A program may use at most 128 MiB of HBM per device.

v0:
```python
import math

import jax
import jax.numpy as jnp
from jax import lax
from jax.sharding import Mesh
from jax.sharding import PartitionSpec as P

HEAD = 64
SP = ("sp_0", "sp_1", "sp_2")
SP_TP = ("sp_0", "sp_1", "sp_2", "tp")


NORM_EPS = 1e-06
GROUP_EPS = 1e-05
HEAD_EPS = 0.00064
KEY_EPS = 1e-06
HIGHEST = lax.Precision.HIGHEST


def from_behind(value, axis, steps):
    count = lax.axis_size(axis)
    leading, last = (max(0, -steps), min(count, count - steps))
    return lax.ppermute(value, axis, [(source, source + steps) for source in range(leading, last)])


def neutral_like(value, identity):
    return jax.tree.map(
        lambda part, zero: jnp.zeros_like(part) + jnp.asarray(zero, part.dtype), value, identity
    )


def entering_2(value, axes, combine, identity):
    before = start = neutral_like(value, identity)
    running = value
    for axis in reversed(axes):
        length, mine = (lax.axis_size(axis), lax.axis_index(axis))
        pieces = jax.tree.map(lambda part: lax.all_gather(part, axis), running)
        inside, running = (start, start)
        for k in range(length):
            passed = k < mine
            running = combine(running, jax.tree.map(lambda part: part[k], pieces))
            inside = jax.tree.map(lambda new, old: jnp.where(passed, new, old), running, inside)
        before = combine(inside, before)
    return before


def stored(values):
    return lax.optimization_barrier(values.astype(jnp.bfloat16)).astype(jnp.float32)


def einsum_exact(form, left, right):
    return jnp.einsum(form, left, right, precision=HIGHEST)


def to_blocks(values, span_len):
    tok_rows, width = values.shape
    return values.reshape(tok_rows // span_len, span_len, width // HEAD, HEAD).transpose(2, 0, 1, 3)


def block_pass(receptance, decay_logarithm, key_rows, value_rows, unit_key, erase_dir):
    span_len = receptance.shape[2]
    cumulate = jnp.cumsum(decay_logarithm, axis=2)
    before = cumulate - decay_logarithm
    final = cumulate[:, :, -1:, :]
    query_unit = unit_key * jnp.exp(before)
    query_read = receptance * jnp.exp(cumulate)
    scaled_erase = erase_dir * jnp.exp(-cumulate)
    scaled_key = key_rows * jnp.exp(-cumulate)
    strict = jnp.tril(jnp.ones((span_len, span_len), jnp.float32), -1)
    inclusive = jnp.tril(jnp.ones((span_len, span_len), jnp.float32))
    erase_mix = einsum_exact("hbsn,hbjn->hbsj", query_unit, scaled_erase) * strict
    key_mix = einsum_exact("hbsn,hbjn->hbsj", query_unit, scaled_key) * strict
    right_side = jnp.concatenate(
        [-einsum_exact("hbsj,hbjn->hbsn", key_mix, value_rows), -query_unit], axis=-1
    )
    system = erase_mix + jnp.eye(span_len, dtype=jnp.float32)
    removed = jax.scipy.linalg.solve_triangular(system, right_side, lower=True, unit_diagonal=True)
    read_erase = einsum_exact("hbtn,hbjn->hbtj", query_read, scaled_erase) * inclusive
    read_key = einsum_exact("hbtn,hbjn->hbtj", query_read, scaled_key) * inclusive
    readout = einsum_exact("hbtj,hbjr->hbtr", read_erase, removed) + jnp.concatenate(
        [einsum_exact("hbtj,hbjn->hbtn", read_key, value_rows), query_read], axis=-1
    )
    kept_erase = erase_dir * jnp.exp(final - cumulate)
    kept_key = key_rows * jnp.exp(final - cumulate)
    from_removed = einsum_exact("hbjr,hbjn->hbrn", removed, kept_erase)
    local_base = from_removed[:, :, :HEAD] + einsum_exact("hbjv,hbjn->hbvn", value_rows, kept_key)
    transfer = from_removed[:, :, HEAD:] + jnp.eye(HEAD, dtype=jnp.float32) * jnp.exp(final)
    return (readout[..., :HEAD], readout[..., HEAD:], transfer, local_base)


def compose(carry, block):
    trans_now, base_now = carry
    block_trans, block_base = block
    joined = (
        einsum_exact("hij,hjk->hik", trans_now, block_trans),
        einsum_exact("hij,hjk->hik", base_now, block_trans) + block_base,
    )
    return (joined, carry)


def chain(earlier, later):
    return (
        einsum_exact("hij,hjk->hik", earlier[0], later[0]),
        einsum_exact("hij,hjk->hik", earlier[1], later[0]) + later[1],
    )


def local(
    tokens,
    input_norm_gain,
    convolution_value_weight,
    convolution_gate_weight,
    depthwise_taps_weight,
    convolution_group_gain,
    convolution_group_shift,
    receptance_weight,
    key_weight,
    value_weight,
    decay_weight,
    correction_rate_weight,
    output_gate_weight,
    key_prenorm_gain,
    decay_offset_bias,
    position_decay_shift,
    extra_log_decay,
    head_norm_gain,
    convolution_output_weight,
    attention_output_weight,
):
    tok_rows = tokens.shape[0]
    float_rows = tokens.astype(jnp.float32)
    normed = (
        float_rows
        * lax.rsqrt(jnp.mean(float_rows * float_rows, axis=-1, keepdims=True) + NORM_EPS)
        * input_norm_gain
    ).astype(jnp.bfloat16)

    def project(weight):
        return stored(jnp.dot(normed, weight, preferred_element_type=jnp.float32))

    conv_input = (
        project(convolution_value_weight) * jax.nn.sigmoid(project(convolution_gate_weight))
    ).astype(jnp.bfloat16)
    tap_count = depthwise_taps_weight.shape[0]
    earlier_rows = from_behind(conv_input[tok_rows - tap_count + 1 :], SP, 1)
    extended = jnp.concatenate([earlier_rows, conv_input], axis=0).astype(jnp.float32)
    conv_sum = jnp.zeros((tok_rows, conv_input.shape[1]), jnp.float32)
    for offset in range(tap_count):
        conv_sum = conv_sum + depthwise_taps_weight[offset] * extended[offset : offset + tok_rows]
    channels = conv_input.shape[1]
    grouped = conv_sum.reshape(tok_rows, channels // 64, 64)
    centred = grouped - jnp.mean(grouped, axis=-1, keepdims=True)
    grouped = centred * lax.rsqrt(jnp.mean(centred * centred, axis=-1, keepdims=True) + GROUP_EPS)
    conv_out = jax.nn.silu(
        grouped.reshape(tok_rows, channels) * convolution_group_gain + convolution_group_shift
    ).astype(jnp.bfloat16)
    span_len = math.gcd(64, tok_rows)
    receptance = project(receptance_weight)
    key_all = project(key_weight)
    value_all = project(value_weight)
    decay_logits = project(decay_weight) + decay_offset_bias + position_decay_shift
    decay_logarithm = -jnp.exp(-jax.nn.softplus(-decay_logits) - 0.5) + extra_log_decay
    erase_rate = jax.nn.sigmoid(project(correction_rate_weight))
    out_gate = jax.nn.sigmoid(project(output_gate_weight))
    unit_key = to_blocks(key_all * key_prenorm_gain, span_len)
    unit_key = unit_key * lax.rsqrt(jnp.sum(unit_key * unit_key, axis=-1, keepdims=True) + KEY_EPS)
    erase_dir = unit_key * to_blocks(erase_rate, span_len)
    local_read, carried_read, transfer, local_base = block_pass(
        to_blocks(receptance, span_len),
        to_blocks(decay_logarithm, span_len),
        to_blocks(key_all, span_len),
        to_blocks(value_all, span_len),
        unit_key,
        erase_dir,
    )
    head_count = transfer.shape[0]
    identity = jnp.broadcast_to(jnp.eye(HEAD, dtype=jnp.float32), (head_count, HEAD, HEAD))
    empty = jnp.zeros((head_count, HEAD, HEAD), jnp.float32)
    totals, priors = lax.scan(
        compose, (identity, empty), (jnp.moveaxis(transfer, 1, 0), jnp.moveaxis(local_base, 1, 0))
    )
    total_trans, total_base = totals
    prior_trans, prior_base = priors
    prefix = entering_2((total_trans, total_base), SP, chain, (identity, empty))
    incoming = prefix[1]
    entering = einsum_exact("hij,bhjk->hbik", incoming, prior_trans) + jnp.moveaxis(
        prior_base, 0, 1
    )
    readout = local_read + einsum_exact("hbtk,hbik->hbti", carried_read, entering)
    centred_read = readout - jnp.mean(readout, axis=-1, keepdims=True)
    normed_read = centred_read * lax.rsqrt(
        jnp.mean(centred_read * centred_read, axis=-1, keepdims=True) + HEAD_EPS
    )
    mix_rows = normed_read.transpose(1, 2, 0, 3).reshape(tok_rows, head_count * HEAD)
    mix_out = (mix_rows * head_norm_gain * out_gate).astype(jnp.bfloat16)
    conv_full, mix_full = (
        lax.all_to_all(conv_out, "tp", split_axis=0, concat_axis=1, tiled=True),
        lax.all_to_all(mix_out, "tp", split_axis=0, concat_axis=1, tiled=True),
    )
    projected = jnp.dot(
        conv_full, convolution_output_weight, preferred_element_type=jnp.float32
    ) + jnp.dot(mix_full, attention_output_weight, preferred_element_type=jnp.float32)
    return projected.astype(jnp.bfloat16)


def solution(mesh):
    split = Mesh(mesh.devices.reshape(4, 4, 2, mesh.shape["tp"]), ("sp_0", "sp_1", "sp_2", "tp"))
    placed = (
        P(SP, None),
        P(),
        P(None, "tp"),
        P(None, "tp"),
        P(None, "tp"),
        P("tp"),
        P("tp"),
        P(None, "tp"),
        P(None, "tp"),
        P(None, "tp"),
        P(None, "tp"),
        P(None, "tp"),
        P(None, "tp"),
        P("tp"),
        P("tp"),
        P(SP, "tp"),
        P(SP, "tp"),
        P("tp"),
        P(),
        P(),
    )
    return jax.shard_map(
        local, mesh=split, in_specs=placed, out_specs=P(SP_TP, None), check_vma=False
    )
```

profile of v0, /device:TPU:96, one launch (start us, length us, event | category | flops | bytes accessed | tf_op | source)
XLA Modules:
  0.0 240.3 jit_solution(9391969910535645362)
XLA Ops:
  0.0 1.7 fusion.12
  1.7 2.0 convolution_convert_fusion.7
  4.3 2.1 collective-permute-start
  8.6 2.0 convolution_convert_fusion.3
  12.2 2.0 convolution_convert_fusion.2
  15.4 2.0 convolution_convert_fusion.5
  18.5 1.5 reduce_window_sum.11
  20.0 2.6 %fusion.160 = (f32[4,4,64,64]{3,2,1,0:T(8,128)}, f32[4,4,64,64]{3,2,1,0:T(8,128)S(1)}, f32[4,4,64,64]{3,2,1,0:T(8,128)S(1)}, f32[4,4,64,64]{3,2,1,0:T(8,128)S(1)}) fusion(f32[4,4,64,64]{3,2,1,0:T(8,128)S(1)} %reduce_window_sum.11, f32[4,64,4,64]{3,2,1,0:T(4,128)} %copy-done.5, f32[4,4,64]{2,1,0:T(4,128)S(1)} %add_rsqrt_fusion.1, ...), kind=kLoop, calls=%fused_computation.282 | loop fusion | flops 393216 | bytes 2363392 | tf_op jit(solution)/shard_map/neg | solution.py:75
  22.6 1.8 convolution_multiply_fusion.3
  24.4 1.8 convolution_multiply_fusion
  26.3 1.8 convolution_multiply_fusion.1
  28.1 1.8 fusion.18
  29.9 80.0 %custom-call.4 = f32[4,4,1,64,64]{3,4,2,1,0:T(8,128)} custom-call(f32[4,4,1,64,64]{4,3,2,1,0:T(8,128)} %fusion.18), custom_call_target="InvertDiagBlocksLowerTriangular" | custom-call | tf_op jit(solution)/shard_map/jit(_solve_triangular)/vmap(vmap())/triangular_solve | solution.py:78
  109.9 2.0 convolution_convert_fusion.1
  114.0 1.7 convolution_negate_fusion
  115.7 2.4 %fusion.25 = f32[4,4,64,128]{3,2,1,0:T(8,128)S(1)} fusion(f32[4,4,64,64]{3,2,1,0:T(8,128)} %get-tuple-element.108, f32[4,4,64,64]{3,2,1,0:T(8,128)S(1)} %convolution_negate_fusion, f32[4,4,1,64,64]{3,4,2,1,0:T(8,128)} %custom-call.4), kind=kOutput, calls=%fused_computation.61 | convolution fusion | flops 100794368 | bytes 1310720 | tf_op jit(solution)/shard_map/jit(_solve_triangular)/vmap(vmap())/triangular_solve | solution.py:78
  119.2 1.4 fusion.20
  123.0 9.9 %while.17 = (s32[]{:T(128)}, f32[4,64,64]{1,2,0:T(8,128)S(1)}, f32[4,64,64]{1,2,0:T(8,128)S(1)}, f32[4,4,64,64]{2,3,1,0:T(8,128)}, f32[4,4,64,64]{2,3,1,0:T(8,12...) while((s32[]{:T(128)}, f32[4,64,64]{1,2,0:T(8,128)S(1)}, ...), condition=%wide.region_6.7_spmd.clone, body=%wide.region_5.6_spmd.clone.sunk | while | flops 25214980 | bytes 1443436 | solution.py:180
  126.3 1.3 fusion.211
  128.8 1.3 fusion.211
  133.1 3.3 %all-gather = f32[8,64,64]{2,1,0:T(8,128)S(1)} all-gather(f32[4,64,64]{2,1,0:T(8,128)S(1)} %copy.95), channel_id=2, replica_groups=mesh['sp_0'=4,'sp_1'=4,'sp_2'=2,'tp'=4] {'sp_2'}, dimensions={0}, use_global_device_ids=true | all-gather | bytes 196608 | tf_op jit(solution)/shard_map/all_gather | solution.py:38
  138.0 13.2 %all-gather.1 = f32[16,64,64]{2,1,0:T(8,128)S(1)} all-gather(f32[4,64,64]{2,1,0:T(8,128)S(1)} %fusion.112), channel_id=3, replica_groups=mesh['sp_0'=4,'sp_1'=4,'sp_2'=2,'tp'=4] {'sp_1'}, dimensions={0}, use_global_device_ids=true | all-gather | bytes 327680 | tf_op jit(solution)/shard_map/all_gather | solution.py:38
  151.9 2.2 all-gather.3
  156.5 13.0 %all-gather.4 = f32[16,64,64]{2,1,0:T(8,128)S(1)} all-gather(f32[4,64,64]{2,1,0:T(8,128)S(1)} %convolution_add_fusion.11), channel_id=6, replica_groups=mesh['sp_0'=4,'sp_1'=4,'sp_2'=2,'tp'=4] {'sp_1'}, dimensions={0}, use_global_device_ids=true | all-gather | bytes 327680 | tf_op jit(solution)/shard_map/all_gather | solution.py:38
  175.9 13.5 %all-gather.2 = f32[16,64,64]{2,1,0:T(8,128)} all-gather(f32[4,64,64]{2,1,0:T(8,128)S(1)} %fusion.100), channel_id=4, replica_groups=mesh['sp_0'=4,'sp_1'=4,'sp_2'=2,'tp'=4] {'sp_0'}, dimensions={0}, use_global_device_ids=true | all-gather | bytes 327680 | tf_op jit(solution)/shard_map/all_gather | solution.py:38
  191.6 13.7 %all-gather.5 = f32[16,64,64]{2,1,0:T(8,128)} all-gather(f32[4,64,64]{2,1,0:T(8,128)S(1)} %copy-done.25), channel_id=7, replica_groups=mesh['sp_0'=4,'sp_1'=4,'sp_2'=2,'tp'=4] {'sp_0'}, dimensions={0}, use_global_device_ids=true | all-gather | bytes 327680 | tf_op jit(solution)/shard_map/all_gather | solution.py:38
  205.3 1.7 fusion.42
  217.0 4.3 %all-to-all-start = ((bf16[4,64,128]{2,1,0:T(8,128)(2,1)}), bf16[4,64,128]{2,1,0:T(8,128)(2,1)S(1)}, u32[]{:S(2)}, u32[]{:S(2)}) async-start(bf16[4,64,128]{2,1,0:T(8,128)(2,1)} %bitcast.34), calls=%async_computation | async-start | bytes 131072 | tf_op jit(solution)/shard_map/all_to_all | solution.py:198
  222.0 5.2 %all-to-all-done = bf16[4,64,128]{2,1,0:T(8,128)(2,1)S(1)} async-done(((bf16[4,64,128]{2,1,0:T(8,128)(2,1)}), bf16[4,64,128]{2,1,0:T(8,128)(2,1)S(1)}, u32[]{:S(2)}, u32[]{:S(2)}) %all-to-all-start) | async-done | bytes 65568 | tf_op jit(solution)/shard_map/all_to_all | solution.py:198
  227.3 3.3 %all-to-all-start.1 = ((bf16[4,64,256]{2,1,0:T(8,128)(2,1)}), bf16[4,64,256]{2,1,0:T(8,128)(2,1)S(1)}, u32[]{:S(2)}, u32[]{:S(2)}) async-start(bf16[4,64,256]{2,1,0:T(8,128)(2,1)} %bitcast.56), calls=%async_computation.1 | async-start | bytes 262144 | tf_op jit(solution)/shard_map/all_to_all | solution.py:199
  231.1 5.4 %all-to-all-done.1 = bf16[4,64,256]{2,1,0:T(8,128)(2,1)S(1)} async-done(((bf16[4,64,256]{2,1,0:T(8,128)(2,1)}), bf16[4,64,256]{2,1,0:T(8,128)(2,1)S(1)}, u32[]{:S(2)}, u32[]{:S(2)}) %all-to-all-start.1) | async-done | bytes 131104 | tf_op jit(solution)/shard_map/all_to_all | solution.py:199
  236.5 3.7 %fusion.11 = bf16[64,2048]{1,0:T(8,128)(2,1)} fusion(f32[64,2048]{1,0:T(8,128)S(1)} %fusion.118, bf16[64,1024]{1,0:T(8,128)(2,1)S(1)} %bitcast.216, bf16[1024,2048]{1,0:T(8,128)(2,1)} %param.41), kind=kOutput, calls=%fused_computation.18 | convolution fusion | flops 268697600 | bytes 5111808 | tf_op jit(solution)/shard_map/dot_general | solution.py:203
  (212 shorter events, 42.9 us)
Async XLA Ops:
  0.0 230.6 %copy-start = (bf16[512,2048]{1,0:T(8,128)(2,1)S(1)}, bf16[512,2048]{1,0:T(8,128)(2,1)}, u32[]{:S(2)}) copy-start(bf16[512,2048]{1,0:T(8,128)(2,1)} %param.40) | copy-start | bytes 6291460
  0.0 3.7 %copy-start.32 = (bf16[256,2048]{1,0:T(8,128)(2,1)S(1)}, bf16[256,2048]{1,0:T(8,128)(2,1)}, u32[]{:S(2)}) copy-start(bf16[256,2048]{1,0:T(8,128)(2,1)} %param.22) | copy-start | bytes 3145732
  0.0 3.7 %copy-start.53 = (f32[2048]{0:T(1024)S(1)}, f32[2048]{0:T(1024)}, u32[]{:S(2)}) copy-start(f32[2048]{0:T(1024)} %param.23) | copy-start | bytes 24580
  0.0 3.7 %copy-start.52 = (bf16[2048,128]{1,0:T(8,128)(2,1)S(1)}, bf16[2048,128]{1,0:T(8,128)(2,1)}, u32[]{:S(2)}) copy-start(bf16[2048,128]{1,0:T(8,128)(2,1)} %param.25) | copy-start | bytes 1572868
  1.7 108.2 %copy-start.45 = (f32[256]{0:T(256)}, f32[256]{0:T(256)S(1)}, u32[]{:S(2)}) copy-start(f32[256]{0:T(256)S(1)} %add_rsqrt_fusion.3) | copy-start | bytes 3076
  1.7 4.9 %copy-start.50 = (bf16[2048,256]{1,0:T(8,128)(2,1)S(1)}, bf16[2048,256]{1,0:T(8,128)(2,1)}, u32[]{:S(2)}) copy-start(bf16[2048,256]{1,0:T(8,128)(2,1)} %param.32) | copy-start | bytes 3145732
  4.3 210.7 %collective-permute-start = (bf16[30,128]{1,0:T(8,128)(2,1)S(1)}, bf16[30,128]{1,0:T(8,128)(2,1)S(1)}, u32[]{:S(2)}, u32[]{:S(2)}) collective-permute-start(bf16[30,128]{1,0:T(8,128)(2,1)S(1)} %slice.378), channel_id=1, source_target_pairs={{0,4},{4,8},{8,12},{12,16},{16,20},{20,24},{24,28},{28,32},{32,36}... | collective-permute-start | bytes 23048 | tf_op jit(solution)/shard_map/ppermute | solution.py:24
  6.5 163.1 %copy-start.11 = (f32[64,64]{1,0:T(8,128)}, f32[64,64]{1,0:T(8,128)S(1)}, u32[]{:S(2)}) copy-start(f32[64,64]{1,0:T(8,128)S(1)} %get-tuple-element.150) | copy-start | bytes 49156
  7.6 3.0 %copy-start.5 = (f32[4,64,4,64]{3,2,1,0:T(4,128)}, f32[4,64,4,64]{3,2,1,0:T(4,128)S(1)}, u32[]{:S(2)}) copy-start(f32[4,64,4,64]{3,2,1,0:T(4,128)S(1)} %reshape.120) | copy-start | bytes 786436
  8.6 3.1 %copy-start.43 = (f32[256]{0:T(256)S(1)}, f32[256]{0:T(256)}, u32[]{:S(2)}) copy-start(f32[256]{0:T(256)} %param.35) | copy-start | bytes 3076
  11.9 3.4 %copy-start.6 = (f32[4,64,4,64]{3,2,1,0:T(4,128)}, f32[4,64,4,64]{3,2,1,0:T(4,128)S(1)}, u32[]{:S(2)}) copy-start(f32[4,64,4,64]{3,2,1,0:T(4,128)S(1)} %reshape.121) | copy-start | bytes 786436
  22.6 5.5 %copy-start.3 = (f32[4,4,64,64]{3,2,1,0:T(8,128)}, f32[4,4,64,64]{3,2,1,0:T(8,128)S(1)}, u32[]{:S(2)}) copy-start(f32[4,4,64,64]{3,2,1,0:T(8,128)S(1)} %get-tuple-element.112) | copy-start | bytes 786436
  114.0 5.2 %copy-start.9 = (bf16[4,64,4,64]{1,3,0,2:T(8,128)(2,1)}, bf16[4,64,4,64]{1,3,0,2:T(8,128)(2,1)S(1)}, u32[]{:S(2)}) copy-start(bf16[4,64,4,64]{1,3,0,2:T(8,128)(2,1)S(1)} %copy.111) | copy-start | bytes 393220
  114.0 4.1 %copy-start.4 = (f32[4,4,64,64]{3,2,1,0:T(8,128)S(1)}, f32[4,4,64,64]{3,2,1,0:T(8,128)}, u32[]{:S(2)}) copy-start(f32[4,4,64,64]{3,2,1,0:T(8,128)} %copy-done.3) | copy-start | bytes 786436
  115.7 3.5 %copy-start.2 = (f32[4,64,4,64]{3,2,1,0:T(4,128)S(1)}, f32[4,64,4,64]{3,2,1,0:T(4,128)}, u32[]{:S(2)}) copy-start(f32[4,64,4,64]{3,2,1,0:T(4,128)} %reshape.123) | copy-start | bytes 786436
  138.0 34.5 %copy-start.18 = (f32[4,64,64]{2,1,0:T(8,128)}, f32[4,64,64]{2,1,0:T(8,128)S(1)}, u32[]{:S(2)}) copy-start(f32[4,64,64]{2,1,0:T(8,128)S(1)} %fusion.112) | copy-start | bytes 196612
  155.3 14.3 %copy-start.21 = (f32[4,64,64]{2,1,0:T(8,128)}, f32[4,64,64]{2,1,0:T(8,128)S(1)}, u32[]{:S(2)}) copy-start(f32[4,64,64]{2,1,0:T(8,128)S(1)} %convolution_add_fusion.12) | copy-start | bytes 196612
  156.5 14.0 %copy-start.23 = (f32[4,64,64]{2,1,0:T(8,128)}, f32[4,64,64]{2,1,0:T(8,128)S(1)}, u32[]{:S(2)}) copy-start(f32[4,64,64]{2,1,0:T(8,128)S(1)} %convolution_add_fusion.11) | copy-start | bytes 196612
  170.5 18.9 %copy-start.12 = (f32[64,64]{1,0:T(8,128)S(1)}, f32[64,64]{1,0:T(8,128)}, u32[]{:S(2)}) copy-start(f32[64,64]{1,0:T(8,128)} %copy-done.11) | copy-start | bytes 49156
  174.1 15.6 %copy-start.20 = (f32[4,64,64]{2,1,0:T(8,128)S(1)}, f32[4,64,64]{2,1,0:T(8,128)}, u32[]{:S(2)}) copy-start(f32[4,64,64]{2,1,0:T(8,128)} %fusion.109) | copy-start | bytes 196612
  174.1 16.5 %copy-start.25 = (f32[4,64,64]{2,1,0:T(8,128)S(1)}, f32[4,64,64]{2,1,0:T(8,128)}, u32[]{:S(2)}) copy-start(f32[4,64,64]{2,1,0:T(8,128)} %convolution_add_fusion.8) | copy-start | bytes 196612
  174.1 16.5 %copy-start.27 = (f32[4,64,64]{2,1,0:T(8,128)S(1)}, f32[4,64,64]{2,1,0:T(8,128)}, u32[]{:S(2)}) copy-start(f32[4,64,64]{2,1,0:T(8,128)} %copy-done.26) | copy-start | bytes 196612
  174.1 16.5 %copy-start.29 = (f32[4,64,64]{2,1,0:T(8,128)S(1)}, f32[4,64,64]{2,1,0:T(8,128)}, u32[]{:S(2)}) copy-start(f32[4,64,64]{2,1,0:T(8,128)} %copy-done.28) | copy-start | bytes 196612
  174.1 16.5 %copy-start.31 = (f32[4,64,64]{2,1,0:T(8,128)S(1)}, f32[4,64,64]{2,1,0:T(8,128)}, u32[]{:S(2)}) copy-start(f32[4,64,64]{2,1,0:T(8,128)} %copy-done.30) | copy-start | bytes 196612
  175.4 30.0 %copy-start.10 = (bf16[4,64,4,64]{1,3,0,2:T(8,128)(2,1)S(1)}, bf16[4,64,4,64]{1,3,0,2:T(8,128)(2,1)}, u32[]{:S(2)}) copy-start(bf16[4,64,4,64]{1,3,0,2:T(8,128)(2,1)} %copy-done.9) | copy-start | bytes 393220
  190.6 19.2 %copy-start.8 = (f32[4,4,64,128]{3,2,1,0:T(8,128)S(1)}, f32[4,4,64,128]{3,2,1,0:T(8,128)}, u32[]{:S(2)}) copy-start(f32[4,4,64,128]{3,2,1,0:T(8,128)} %copy-done.7) | copy-start | bytes 1572868
  205.3 4.2 %copy-start.16 = (f32[16,64,64]{2,1,0:T(8,128)S(1)}, f32[16,64,64]{2,1,0:T(8,128)}, u32[]{:S(2)}) copy-start(f32[16,64,64]{2,1,0:T(8,128)} %all-gather.2) | copy-start | bytes 786436
  205.3 4.2 %copy-start.17 = (f32[16,64,64]{2,1,0:T(8,128)S(1)}, f32[16,64,64]{2,1,0:T(8,128)}, u32[]{:S(2)}) copy-start(f32[16,64,64]{2,1,0:T(8,128)} %all-gather.5) | copy-start | bytes 786436
  205.3 4.5 %copy-start.15 = (f32[4,4,64,64]{3,2,1,0:T(8,128)S(1)}, f32[4,4,64,64]{3,2,1,0:T(8,128)}, u32[]{:S(2)}) copy-start(f32[4,4,64,64]{3,2,1,0:T(8,128)} %convolution_multiply_fusion.3) | copy-start | bytes 786436
  215.9 5.4 %copy-start.44 = (f32[256]{0:T(256)S(1)}, f32[256]{0:T(256)}, u32[]{:S(2)}) copy-start(f32[256]{0:T(256)} %param.39) | copy-start | bytes 3076
  217.0 10.3 %all-to-all-start = ((bf16[4,64,128]{2,1,0:T(8,128)(2,1)}), bf16[4,64,128]{2,1,0:T(8,128)(2,1)S(1)}, u32[]{:S(2)}, u32[]{:S(2)}) async-start(bf16[4,64,128]{2,1,0:T(8,128)(2,1)} %bitcast.34), calls=%async_computation | async-start | bytes 131072 | tf_op jit(solution)/shard_map/all_to_all | solution.py:198
  227.3 9.3 %all-to-all-start.1 = ((bf16[4,64,256]{2,1,0:T(8,128)(2,1)}), bf16[4,64,256]{2,1,0:T(8,128)(2,1)S(1)}, u32[]{:S(2)}, u32[]{:S(2)}) async-start(bf16[4,64,256]{2,1,0:T(8,128)(2,1)} %bitcast.56), calls=%async_computation.1 | async-start | bytes 262144 | tf_op jit(solution)/shard_map/all_to_all | solution.py:199
  (26 other events, 42.1 us)
where the time goes:
time: 243 us; the launch traced here: 240 us
  other arithmetic  93.6 us (39%)
  blocking collectives  59 us (24%)
  matrix products  53 us (22%)
  local copies, waits for them, and re-layouts  13.1 us (5%)
  waiting for transfers between devices  10.7 us (4%)
  starting transfers between devices  9.67 us (4%)
    another operation x6, other arithmetic, block_pass(): jax.scipy.linalg.solve_triangular(system, right_side, lower=True, unit_di...  80.1 us
    all_gather x6, blocking collectives, entering_2(): pieces = jax.tree.map(lambda part: lax.all_gather(part, axis), running)  59 us
    dot_general x40, matrix products, einsum_exact(): return jnp.einsum(form, left, right, precision=HIGHEST)  34.8 us
    dot_general x8, matrix products, project(): return stored(jnp.dot(normed, weight, preferred_element_type=jnp.float32))  11.6 us
    all_to_all x1, waiting for transfers between devices, local(): lax.all_to_all(mix_out, 'tp', split_axis=0, concat_axis=1, tiled=True)  5.45 us
    all_to_all x1, waiting for transfers between devices, local(): lax.all_to_all(conv_out, 'tp', split_axis=0, concat_axis=1, tiled=True)  5.24 us
  transfers between devices with their start and end apart: 3, of which 2 were waited for; matrix products, arithmetic and copies ran while one was open for 61% of the time, Pallas kernels for 0%

commit v1 on v0

v1 whole, which is shorter than its diff:
```python
import functools

import jax
import jax.numpy as jnp
from jax import lax
from jax.experimental import pallas as pl
from jax.experimental.pallas import tpu as pltpu
from jax.sharding import PartitionSpec as P

F32 = jnp.float32
BF16 = jnp.bfloat16
MESH = pl.DeviceIdType.MESH
HEAD = 64
CHUNK = 64
PAIR = 128

NORM_EPS = 1e-06
GROUP_EPS = 1e-05
HEAD_EPS = 0.00064
KEY_EPS = 1e-06

NN = (((1,), (0,)), ((), ()))
NT = (((1,), (1,)), ((), ()))


def dot(left, right, dims=NN):
    return lax.dot_general(left, right, dims, preferred_element_type=F32)


def split(values):
    high = values.astype(BF16)
    return high, (values - high.astype(F32)).astype(BF16)


def dot1(left, right, dims=NN):
    return dot(left.astype(BF16), right.astype(BF16), dims)


def dot3(left, right, dims=NN):
    left_high, left_low = split(left)
    right_high, right_low = split(right)
    return dot(left_high, right_high, dims) + (
        dot(left_low, right_high, dims) + dot(left_high, right_low, dims)
    )


def dot2(left, right_exact):
    high, low = split(left)
    return dot(high, right_exact) + dot(low, right_exact)


def iota(shape, dim):
    return lax.broadcasted_iota(jnp.int32, shape, dim)


def first_head(rows):
    return iota((rows, PAIR), 1) < HEAD


def diagonal(packed):
    mask = first_head(packed.shape[0])
    return jnp.concatenate([jnp.where(mask, packed, 0.0), jnp.where(mask, 0.0, packed)], axis=0)


def undiagonal(full):
    return jnp.where(first_head(HEAD), full[:HEAD], full[HEAD:])


def beside(*parts):
    return jnp.concatenate(parts, axis=1)


def group_ones(width):
    return (iota((width, width), 0) // HEAD == iota((width, width), 1) // HEAD).astype(BF16)


def sigmoid(values):
    return 1.0 / (1.0 + jnp.exp(-values))


def rounded(values):
    return values.astype(BF16).astype(F32)


def normalize(tokens, gain):
    rows = tokens.astype(F32)
    scale = lax.rsqrt(jnp.mean(rows * rows, axis=-1, keepdims=True) + NORM_EPS)
    return (rows * scale * gain).astype(BF16)


def group_norm(values, ones, eps):
    centred = values - dot2(values, ones) * (1.0 / HEAD)
    return centred * lax.rsqrt(dot2(centred * centred, ones) * (1.0 / HEAD) + eps)


def compose(later, earlier, product):
    trans, base = later
    out = product(trans, beside(diagonal(earlier[0]), diagonal(earlier[1])))
    return out[:, :PAIR], out[:, PAIR:] + base


def chunk_algebra(receptance, key, value, decay, rate, key_gain, decay_bias, shift, extra):
    tok_rows, width = receptance.shape
    chunks, pairs = tok_rows // CHUNK, width // PAIR
    logits = decay + decay_bias + shift
    log_decay = sigmoid(logits) * (-0.6065306597126334) + extra
    scaled = key * key_gain
    ones = group_ones(width)
    unit = scaled * lax.rsqrt(dot2(scaled * scaled, ones) + KEY_EPS)
    erase = unit * sigmoid(rate)
    row, col = iota((tok_rows, tok_rows), 0), iota((tok_rows, tok_rows), 1)
    running = ((row // CHUNK == col // CHUNK) & (row >= col)).astype(BF16)
    high, low = split(log_decay)
    total = dot(running, high) + dot(running, low)

    strict_rows = iota((CHUNK, PAIR), 0)
    strict_cols = iota((CHUNK, PAIR), 1) % HEAD
    strict = strict_rows > strict_cols
    inclusive = strict_rows >= strict_cols
    eye = (strict_rows == strict_cols).astype(F32)
    same8 = (strict_rows // 8) == (strict_cols // 8)
    lane_first = first_head(CHUNK)

    units = []
    for c in range(chunks):
        rows = slice(c * CHUNK, (c + 1) * CHUNK)
        cum = total[rows]
        last = cum[CHUNK - 1 : CHUNK]
        half = 0.5 * last
        grow = jnp.exp(half - cum)
        shrink = jnp.exp(cum - half)
        half_decay = jnp.exp(half)
        query_unit = unit[rows] * jnp.exp(cum - log_decay[rows] - half)
        query_read = receptance[rows] * shrink
        scaled_erase = erase[rows] * grow
        scaled_key = key[rows] * grow
        for p in range(pairs):
            lanes = slice(p * PAIR, (p + 1) * PAIR)
            units.append(
                dict(
                    c=c,
                    p=p,
                    qu=query_unit[:, lanes],
                    qr=query_read[:, lanes],
                    se=scaled_erase[:, lanes],
                    sk=scaled_key[:, lanes],
                    v=value[rows, lanes],
                    half=half_decay[:, lanes],
                )
            )
    for u in units:
        left = jnp.concatenate([u["qu"], u["qr"]], axis=0)
        right = jnp.concatenate([diagonal(u["se"]), diagonal(u["sk"])], axis=0)
        u["gram"] = dot3(left, right, NT)
    for u in units:
        gram = u.pop("gram")
        u["mix"] = jnp.where(strict, gram[:CHUNK, :PAIR], 0.0)
        u["key_mix"] = jnp.where(strict, gram[:CHUNK, PAIR:], 0.0)
        u["read_erase"] = jnp.where(inclusive, gram[CHUNK:, :PAIR], 0.0)
        u["read_key"] = jnp.where(inclusive, gram[CHUNK:, PAIR:], 0.0)
        u["near"] = jnp.where(same8, u["mix"], 0.0)
        u["far"] = jnp.where(same8, 0.0, u["mix"])
    for u in units:
        u["near2"] = dot3(u["near"], diagonal(u["near"]))
        u["value_part"] = dot3(
            jnp.concatenate([u.pop("key_mix"), u.pop("read_key")], axis=0), diagonal(u["v"])
        )
    for u in units:
        powers = dot3(jnp.concatenate([u["near"], u["near2"]], axis=0), diagonal(u["near2"]))
        u["start"] = eye - u.pop("near") + u.pop("near2") - powers[:CHUNK]
        u["near4"] = powers[CHUNK:]
    for u in units:
        u["inv8"] = u["start"] + dot3(u["start"], diagonal(u.pop("near4")))
        u.pop("start")
    for u in units:
        u["step"] = dot3(u["inv8"], diagonal(u.pop("far")))
    for u in units:
        out = dot3(u["step"], beside(diagonal(u["step"]), diagonal(u["inv8"])))
        u["step2"] = out[:, :PAIR]
        u["inv"] = u.pop("inv8") - out[:, PAIR:]
        u.pop("step")
    for u in units:
        out = dot3(u["step2"], beside(diagonal(u["step2"]), diagonal(u["inv"])))
        u["step4"] = out[:, :PAIR]
        u["inv"] = u["inv"] + out[:, PAIR:]
        u.pop("step2")
    for u in units:
        u["inv"] = u["inv"] + dot3(u.pop("step4"), diagonal(u["inv"]))
    for u in units:
        right = beside(diagonal(u["value_part"][:CHUNK]), diagonal(u["qu"] * u["half"]))
        u["removed"] = -dot3(u.pop("inv"), right)
    for u in units:
        kept = jnp.concatenate([u["se"] * u["half"], u["sk"] * u["half"]], axis=0)
        right = jnp.concatenate(
            [u["removed"], beside(u["v"], jnp.zeros_like(u["v"]))], axis=0
        )
        out = dot3(kept.T, right)
        u["base"] = undiagonal(out[:, :PAIR])
        u["trans"] = undiagonal(out[:, PAIR:]) + eye * (u["half"] * u["half"])
    for u in units:
        removed = u["removed"]
        right = beside(diagonal(removed[:, :PAIR]), diagonal(removed[:, PAIR:]))
        out = dot3(u["read_erase"], right)
        u["local"] = out[:, :PAIR] + u["value_part"][CHUNK:]
        u["carried"] = out[:, PAIR:] + u["qr"] * u["half"]
    return units


def chunk_prefixes(units, pairs, chunks):
    found = []
    for p in range(pairs):
        steps = [(u["trans"], u["base"]) for u in units if u["p"] == p]
        one = steps[0]
        two = compose(steps[1], one, dot3)
        upper = compose(steps[3], steps[2], dot3)
        three = compose(steps[2], two, dot3)
        found.append([one, two, three, compose(upper, two, dot3)])
    return found


def local_kernel(
    tokens_hbm, gain_ref, decay_hbm, key_hbm, rate_hbm, receptance_hbm, value_hbm,
    key_gain_ref, bias_ref, shift_hbm, extra_hbm,
    normed_hbm, total_ref, prefix_ref, local_ref, carried_ref,
    tokens, normed, weights, shift, extra, sems,
):
    order = (decay_hbm, key_hbm, rate_hbm, receptance_hbm, value_hbm)
    copies = [pltpu.make_async_copy(tokens_hbm, tokens, sems.at[0])]
    for i, source in enumerate(order):
        copies.append(pltpu.make_async_copy(source, weights.at[i], sems.at[1 + i]))
    copies.append(pltpu.make_async_copy(shift_hbm, shift, sems.at[6]))
    copies.append(pltpu.make_async_copy(extra_hbm, extra, sems.at[7]))
    for copy in copies:
        copy.start()
    copies[0].wait()
    normed[...] = normalize(tokens[...], gain_ref[...])
    out_copy = pltpu.make_async_copy(normed, normed_hbm, sems.at[8])
    out_copy.start()
    found = []
    for i in range(5):
        copies[1 + i].wait()
        found.append(rounded(dot(normed[...], weights[i])))
    decay, key, rate, receptance, value = found
    copies[6].wait()
    copies[7].wait()
    units = chunk_algebra(
        receptance, key, value, decay, rate, key_gain_ref[...], bias_ref[...], shift[...], extra[...]
    )
    chunks, pairs = 4, 2
    prefixes = chunk_prefixes(units, pairs, chunks)
    for p in range(pairs):
        total_ref[p] = beside(*prefixes[p][3])
        for k in range(3):
            prefix_ref[p, k] = beside(*prefixes[p][k])
    for u in units:
        rows = slice(u["c"] * CHUNK, (u["c"] + 1) * CHUNK)
        lanes = slice(u["p"] * PAIR, (u["p"] + 1) * PAIR)
        local_ref[rows, lanes] = u["local"]
        carried_ref[rows, lanes] = u["carried"]
    out_copy.wait()


def finish_kernel(
    total_ref, prefix_ref, local_ref, carried_ref, normed_hbm,
    conv_value_hbm, conv_gate_hbm, gate_hbm, taps_ref, group_gain_ref, group_shift_ref,
    head_gain_ref, conv_out_hbm, mix_out_hbm,
    out_ref,
    normed, conv_w, gate_w, conv_out_w, mix_out_w,
    peer_total, pair_states, y_slots, z_slots, extended, halo, conv_rows, mix_rows,
    conv_full, mix_full, acc,
    load_sems, pair_send, pair_recv, y_send, y_recv, z_send, z_recv, halo_send, halo_recv,
    conv_send, conv_recv, mix_send, mix_recv,
):
    sp, tp = lax.axis_index("sp"), lax.axis_index("tp")
    core = lax.rem(sp, 2)
    y = lax.rem(sp // 2, 4)
    z = sp // 8
    sibling = sp + 1 - 2 * core
    after, before = lax.rem(sp + 1, 32), lax.rem(sp + 31, 32)

    def y_of(step):
        return lax.rem(y + step, 4)

    def z_of(step):
        return lax.rem(z + step, 4)

    def x_of(step):
        return lax.rem(tp + step, 4)

    def y_peer(step):
        return (z * 8 + y_of(step) * 2 + core, tp)

    def z_peer(step):
        return (z_of(step) * 8 + y * 2 + core, tp)

    def x_peer(step):
        return (sp, x_of(step))

    loads = [
        pltpu.make_async_copy(normed_hbm, normed, load_sems.at[0]),
        pltpu.make_async_copy(conv_value_hbm, conv_w.at[0], load_sems.at[1]),
        pltpu.make_async_copy(conv_gate_hbm, conv_w.at[1], load_sems.at[2]),
        pltpu.make_async_copy(gate_hbm, gate_w, load_sems.at[3]),
        pltpu.make_async_copy(conv_out_hbm, conv_out_w, load_sems.at[4]),
        pltpu.make_async_copy(mix_out_hbm, mix_out_w, load_sems.at[5]),
    ]
    for load in loads:
        load.start()

    barrier = pltpu.get_barrier_semaphore()
    peers = [(sibling, tp), (after, tp), (before, tp)]
    for step in (1, 2, 3):
        peers += [y_peer(step), z_peer(step), x_peer(step)]
    for peer in peers:
        pl.semaphore_signal(barrier, inc=1, device_id=peer, device_id_type=MESH)
    pl.semaphore_wait(barrier, len(peers))

    def remote(source, target, send, recv, peer):
        return pltpu.make_async_remote_copy(
            src_ref=source, dst_ref=target, send_sem=send, recv_sem=recv,
            device_id=peer, device_id_type=MESH,
        )

    pair_copy = remote(
        total_ref.at[1 - core], peer_total, pair_send.at[0], pair_recv.at[0], (sibling, tp)
    )
    pair_copy.start()

    loads[0].wait()
    loads[1].wait()
    conv_value = rounded(dot(normed[...], conv_w[0]))
    loads[2].wait()
    conv_gate = rounded(dot(normed[...], conv_w[1]))
    conv_input = (conv_value * sigmoid(conv_gate)).astype(BF16)
    conv_rows[...] = conv_input[224:]
    halo_copy = remote(conv_rows, halo, halo_send.at[0], halo_recv.at[0], (after, tp))
    halo_copy.start()
    extended[32:, :] = conv_input.astype(F32)

    pair_copy.wait()
    own, other = total_ref[core], peer_total[...]
    is_first = core == 0
    first = jnp.where(is_first, own, other)
    second = jnp.where(is_first, other, own)
    chip_first = (first[:, :PAIR], first[:, PAIR:])
    chip = compose((second[:, :PAIR], second[:, PAIR:]), chip_first, dot3)
    y_slots[y] = beside(*chip).astype(BF16)
    y_copies = []
    for step in (1, 2, 3):
        copy = remote(
            y_slots.at[y], y_slots.at[y], y_send.at[step - 1], y_recv.at[step - 1], y_peer(step)
        )
        copy.start()
        y_copies.append(copy)

    loads[3].wait()
    out_gate = sigmoid(rounded(dot(normed[...], gate_w[...])))
    gate_gain = out_gate * head_gain_ref[...]
    local_rows, carried_rows = [], []
    for p in range(2):
        lanes = slice(p * PAIR, (p + 1) * PAIR)
        local_parts, carried_parts = [local_ref[:CHUNK, lanes]], [carried_ref[:CHUNK, lanes]]
        for c in range(1, 4):
            rows = slice(c * CHUNK, (c + 1) * CHUNK)
            earlier = prefix_ref[p, c - 1]
            out = dot3(
                carried_ref[rows, lanes],
                beside(diagonal(earlier[:, :PAIR]), diagonal(earlier[:, PAIR:])),
            )
            carried_parts.append(out[:, :PAIR])
            local_parts.append(out[:, PAIR:] + local_ref[rows, lanes])
        local_rows.append(jnp.concatenate(local_parts, axis=0))
        carried_rows.append(jnp.concatenate(carried_parts, axis=0))

    for step in (1, 2, 3):
        copy = y_copies[step - 1]
        copy.wait_send()
        arrived = y_of(4 - step)
        remote(
            y_slots.at[arrived], y_slots.at[arrived], y_send.at[step - 1], y_recv.at[step - 1],
            y_peer(step),
        ).wait_recv()

    def slot(ref, k):
        both = ref[k].astype(F32)
        return both[:, :PAIR], both[:, PAIR:]

    c0, c1, c2, c3 = (slot(y_slots, k) for k in range(4))
    c01, c23 = compose(c1, c0, dot1), compose(c3, c2, dot1)
    plane = compose(c23, c01, dot3)
    z_slots[z] = beside(*plane).astype(BF16)
    z_copies = []
    for step in (1, 2, 3):
        copy = remote(
            z_slots.at[z], z_slots.at[z], z_send.at[step - 1], z_recv.at[step - 1], z_peer(step)
        )
        copy.start()
        z_copies.append(copy)
    c012 = compose(c2, c01, dot3)
    eye = (iota((HEAD, PAIR), 0) == iota((HEAD, PAIR), 1) % HEAD).astype(F32)

    def pick(index, a, b, c, d):
        return jnp.where(index == 0, a, jnp.where(index == 1, b, jnp.where(index == 2, c, d)))

    before_chip = (
        pick(y, eye, c0[0], c01[0], c012[0]),
        pick(y, jnp.zeros_like(eye), c0[1], c01[1], c012[1]),
    )
    before_second = compose(chip_first, before_chip, dot3)
    trans_both = jnp.concatenate([before_chip[0], before_second[0]], axis=0)
    base_both = jnp.concatenate([before_chip[1], before_second[1]], axis=0)

    halo_copy.wait()
    extended[:32, :] = jnp.where(sp == 0, 0.0, halo[...].astype(F32))
    taps = taps_ref[...]
    conv_sum = jnp.zeros((256, PAIR), F32)
    for j in range(31):
        conv_sum = conv_sum + taps[j : j + 1] * extended[pl.ds(2 + j, 256), :]
    ones_pair = group_ones(PAIR)
    affine = group_norm(conv_sum, ones_pair, GROUP_EPS) * group_gain_ref[...] + group_shift_ref[...]
    conv_out = (affine * sigmoid(affine)).astype(BF16)
    for k in range(4):
        conv_full[0, k] = conv_out[k * 64 : (k + 1) * 64]
    conv_copies = []
    for step in (1, 2, 3):
        copy = remote(
            conv_full.at[0, x_of(step)], conv_full.at[1, tp],
            conv_send.at[step - 1], conv_recv.at[step - 1], x_peer(step),
        )
        copy.start()
        conv_copies.append(copy)

    for step in (1, 2, 3):
        z_copies[step - 1].wait_send()
        arrived = z_of(4 - step)
        remote(
            z_slots.at[arrived], z_slots.at[arrived], z_send.at[step - 1], z_recv.at[step - 1],
            z_peer(step),
        ).wait_recv()
    p0, p1, p2 = (slot(z_slots, k) for k in range(3))
    into1 = p0[1]
    into2 = dot1(p1[0], diagonal(into1)) + p1[1]
    into3 = dot3(p2[0], diagonal(into2)) + p2[1]
    entering = pick(z, jnp.zeros_like(into1), into1, into2, into3)
    states = dot3(trans_both, diagonal(entering)) + base_both
    state_first, state_second = states[:HEAD], states[HEAD:]
    mine = jnp.where(is_first, state_first, state_second)
    pair_states[0] = jnp.where(is_first, state_second, state_first)
    state_copy = remote(
        pair_states.at[0], pair_states.at[1], pair_send.at[1], pair_recv.at[1], (sibling, tp)
    )
    state_copy.start()

    loads[4].wait()
    acc[...] = dot(conv_full[0, tp], conv_out_w[pl.ds(pl.multiple_of(tp * PAIR, PAIR), PAIR), :])
    for step in (1, 2, 3):
        conv_copies[step - 1].wait_send()
        arrived = x_of(4 - step)
        remote(
            conv_full.at[0, arrived], conv_full.at[1, arrived],
            conv_send.at[step - 1], conv_recv.at[step - 1], x_peer(step),
        ).wait_recv()
        rows = pl.ds(pl.multiple_of(arrived * PAIR, PAIR), PAIR)
        acc[...] += dot(conv_full[1, arrived], conv_out_w[rows, :])

    state_copy.wait()
    theirs = pair_states[1]
    state_pairs = (jnp.where(is_first, mine, theirs), jnp.where(is_first, theirs, mine))
    readout = beside(
        *(local_rows[p] + dot3(carried_rows[p], diagonal(state_pairs[p])) for p in range(2))
    )
    mix_out = (group_norm(readout, group_ones(256), HEAD_EPS) * gate_gain).astype(BF16)
    for k in range(4):
        mix_full[0, k] = mix_out[k * 64 : (k + 1) * 64]
    mix_copies = []
    for step in (1, 2, 3):
        copy = remote(
            mix_full.at[0, x_of(step)], mix_full.at[1, tp],
            mix_send.at[step - 1], mix_recv.at[step - 1], x_peer(step),
        )
        copy.start()
        mix_copies.append(copy)
    loads[5].wait()
    acc[...] += dot(mix_full[0, tp], mix_out_w[pl.ds(pl.multiple_of(tp * 256, 256), 256), :])
    for step in (1, 3, 2):
        mix_copies[step - 1].wait_send()
        arrived = x_of(4 - step)
        remote(
            mix_full.at[0, arrived], mix_full.at[1, arrived],
            mix_send.at[step - 1], mix_recv.at[step - 1], x_peer(step),
        ).wait_recv()
        rows = pl.ds(pl.multiple_of(arrived * 256, 256), 256)
        acc[...] += dot(mix_full[1, arrived], mix_out_w[rows, :])
    out_ref[...] = acc[...].astype(BF16)


VMEM = pl.BlockSpec(memory_space=pltpu.VMEM)
ANY = pl.BlockSpec(memory_space=pl.ANY)


def local(
    tokens, input_norm_gain, convolution_value_weight, convolution_gate_weight,
    depthwise_taps_weight, convolution_group_gain, convolution_group_shift, receptance_weight,
    key_weight, value_weight, decay_weight, correction_rate_weight, output_gate_weight,
    key_prenorm_gain, decay_offset_bias, position_decay_shift, extra_log_decay, head_norm_gain,
    convolution_output_weight, attention_output_weight,
):
    normed, total, prefix, local_read, carried = pl.pallas_call(
        local_kernel,
        name="local_part",
        out_shape=(
            jax.ShapeDtypeStruct((256, 2048), BF16),
            jax.ShapeDtypeStruct((2, 64, 256), F32),
            jax.ShapeDtypeStruct((2, 3, 64, 256), F32),
            jax.ShapeDtypeStruct((256, 256), F32),
            jax.ShapeDtypeStruct((256, 256), F32),
        ),
        in_specs=[ANY, VMEM, ANY, ANY, ANY, ANY, ANY, VMEM, VMEM, ANY, ANY],
        out_specs=(ANY, VMEM, VMEM, VMEM, VMEM),
        scratch_shapes=[
            pltpu.VMEM((256, 2048), BF16),
            pltpu.VMEM((256, 2048), BF16),
            pltpu.VMEM((5, 2048, 256), BF16),
            pltpu.VMEM((256, 256), F32),
            pltpu.VMEM((256, 256), F32),
            pltpu.SemaphoreType.DMA((9,)),
        ],
    )(
        tokens, input_norm_gain.reshape(1, -1), decay_weight, key_weight, correction_rate_weight,
        receptance_weight, value_weight, key_prenorm_gain.reshape(1, -1),
        decay_offset_bias.reshape(1, -1), position_decay_shift, extra_log_decay,
    )
    dma = pltpu.SemaphoreType.DMA
    return pl.pallas_call(
        finish_kernel,
        name="finish_part",
        out_shape=jax.ShapeDtypeStruct((64, 2048), BF16),
        in_specs=[VMEM, VMEM, VMEM, VMEM, ANY, ANY, ANY, ANY, VMEM, VMEM, VMEM, VMEM, ANY, ANY],
        out_specs=VMEM,
        scratch_shapes=[
            pltpu.VMEM((256, 2048), BF16),
            pltpu.VMEM((2, 2048, 128), BF16),
            pltpu.VMEM((2048, 256), BF16),
            pltpu.VMEM((512, 2048), BF16),
            pltpu.VMEM((1024, 2048), BF16),
            pltpu.VMEM((64, 256), F32),
            pltpu.VMEM((2, 64, 128), F32),
            pltpu.VMEM((4, 64, 256), BF16),
            pltpu.VMEM((4, 64, 256), BF16),
            pltpu.VMEM((288, 128), F32),
            pltpu.VMEM((32, 128), BF16),
            pltpu.VMEM((32, 128), BF16),
            pltpu.VMEM((8, 128), BF16),
            pltpu.VMEM((2, 4, 64, 128), BF16),
            pltpu.VMEM((2, 4, 64, 256), BF16),
            pltpu.VMEM((64, 2048), F32),
            dma((6,)), dma((2,)), dma((2,)), dma((3,)), dma((3,)), dma((3,)), dma((3,)),
            dma((1,)), dma((1,)), dma((3,)), dma((3,)), dma((3,)), dma((3,)),
        ],
        compiler_params=pltpu.CompilerParams(collective_id=0, has_side_effects=True),
    )(
        total, prefix, local_read, carried, normed,
        convolution_value_weight, convolution_gate_weight, output_gate_weight,
        depthwise_taps_weight, convolution_group_gain.reshape(1, -1),
        convolution_group_shift.reshape(1, -1), head_norm_gain.reshape(1, -1),
        convolution_output_weight, attention_output_weight,
    )


def solution(mesh):
    rows, chans, vec = P("sp", None), P(None, "tp"), P("tp")
    placed = (
        rows, P(), chans, chans, chans, vec, vec, chans, chans, chans, chans, chans, chans,
        vec, vec, P("sp", "tp"), P("sp", "tp"), vec, P(), P(),
    )
    return jax.shard_map(
        local, mesh=mesh, in_specs=placed, out_specs=P(("sp", "tp"), None), check_vma=False
    )
```

time: 243 us -> 38.9 us (0.16)
  the two profiles are of different devices: /device:TPU:96 before, /device:TPU:1 now
where the time goes in v1:
time: 38.9 us; the launch traced here: 38.7 us
  Pallas kernels  37 us (95%)
  local copies, waits for them, and re-layouts  1.67 us (4%)
    pallas_call x1, Pallas kernels, local(): pl.pallas_call(finish_kernel, name='finish_part', out_shape=jax.ShapeDtyp...  26.1 us
    pallas_call x1, Pallas kernels, local(): pl.pallas_call(local_kernel, name='local_part', out_shape=(jax.ShapeDtype...  10.9 us
    unnamed x1, local copies, waits for them, and re-layouts  1.67 us

profile of v1, /device:TPU:1, one launch (start us, length us, event | category | flops | bytes accessed | tf_op | source)
XLA Modules:
  0.0 38.7 jit_solution(9058143773611331120)
XLA Ops:
  0.0 10.9 %local_part.1 = (bf16[256,2048]{1,0:T(8,128)(2,1)}, f32[2,64,256]{2,1,0:T(8,128)}, f32[2,3,64,256]{3,2,1,0:T(8,128)}, f32[256,256]{1,0:T(8,128)}, f32[256,256]{1,0:T(8,128)}) custom-call(bf16[256,2048]{1,0:T(8,128)(2,1)} %tokens_hbm.1, f32[1,2048]{1,0:T(1,128)} %bitcast.6, bf16[2048,256]{1,0:T(8,128)(2,1)} %decay_hbm.1, bf16[2048,256]{1,0:T(8,128)(2,1)} %key_hbm.1, ...), custom_call_target="tpu_custom_call" | custom-call | tf_op jit(solution)/shard_map/local_part/pallas_call | solution.py:508
  11.0 26.1 %finish_part.1 = bf16[64,2048]{1,0:T(8,128)(2,1)} custom-call(f32[2,64,256]{2,1,0:T(8,128)} %get-tuple-element.10.total_ref, f32[2,3,64,256]{3,2,1,0:T(8,128)} %get-tuple-element.11.prefix_ref, f32[256,256]{1,0:T(8,128)} %get-tuple-element.12.local_ref, f32[256,256]{1,0:T(8,128)} %get-tuple-element.13.carried_ref, ...), custom_call_target="tpu_custom_call" | custom-call | tf_op jit(solution)/shard_map/finish_part/pallas_call | solution.py:534
  37.1 1.7 %copy.22 = bf16[64,2048]{1,0:T(8,128)(2,1)} copy(bf16[64,2048]{1,0:T(8,128)(2,1)} %finish_part.1) | data formatting | bytes 524288

commit v2 on v1

v2 whole, which is shorter than its diff:
```python
import functools

import jax
import jax.numpy as jnp
from jax import lax
from jax.experimental import pallas as pl
from jax.experimental.pallas import tpu as pltpu
from jax.sharding import PartitionSpec as P

F32 = jnp.float32
BF16 = jnp.bfloat16
MESH = pl.DeviceIdType.MESH
HEAD = 64
CHUNK = 64
PAIR = 128

NORM_EPS = 1e-06
GROUP_EPS = 1e-05
HEAD_EPS = 0.00064
KEY_EPS = 1e-06

NN = (((1,), (0,)), ((), ()))
NT = (((1,), (1,)), ((), ()))


def dot(left, right, dims=NN):
    return lax.dot_general(left, right, dims, preferred_element_type=F32)


def split(values):
    high = values.astype(BF16)
    return high, (values - high.astype(F32)).astype(BF16)


def dot1(left, right, dims=NN):
    return dot(left.astype(BF16), right.astype(BF16), dims)


def dot3(left, right, dims=NN):
    left_high, left_low = split(left)
    right_high, right_low = split(right)
    return dot(left_high, right_high, dims) + (
        dot(left_low, right_high, dims) + dot(left_high, right_low, dims)
    )


def dot2(left, right_exact):
    high, low = split(left)
    return dot(high, right_exact) + dot(low, right_exact)


def iota(shape, dim):
    return lax.broadcasted_iota(jnp.int32, shape, dim)


def first_head(rows):
    return iota((rows, PAIR), 1) < HEAD


def diagonal(packed):
    mask = first_head(packed.shape[0])
    return jnp.concatenate([jnp.where(mask, packed, 0.0), jnp.where(mask, 0.0, packed)], axis=0)


def undiagonal(full):
    return jnp.where(first_head(HEAD), full[:HEAD], full[HEAD:])


def beside(*parts):
    return jnp.concatenate(parts, axis=1)


def group_ones(width):
    return (iota((width, width), 0) // HEAD == iota((width, width), 1) // HEAD).astype(BF16)


def sigmoid(values):
    return 1.0 / (1.0 + jnp.exp(-values))


def rounded(values):
    return values.astype(BF16).astype(F32)


def normalize(tokens, gain):
    rows = tokens.astype(F32)
    scale = lax.rsqrt(jnp.mean(rows * rows, axis=-1, keepdims=True) + NORM_EPS)
    return (rows * scale * gain).astype(BF16)


def group_norm(values, ones, eps):
    centred = values - dot2(values, ones) * (1.0 / HEAD)
    return centred * lax.rsqrt(dot2(centred * centred, ones) * (1.0 / HEAD) + eps)


def compose(later, earlier, product):
    trans, base = later
    out = product(trans, beside(diagonal(earlier[0]), diagonal(earlier[1])))
    return out[:, :PAIR], out[:, PAIR:] + base


def chunk_algebra(receptance, key, value, decay, rate, key_gain, decay_bias, shift, extra):
    tok_rows, width = receptance.shape
    chunks, pairs = tok_rows // CHUNK, width // PAIR
    logits = decay + decay_bias + shift
    log_decay = sigmoid(logits) * (-0.6065306597126334) + extra
    scaled = key * key_gain
    ones = group_ones(width)
    unit = scaled * lax.rsqrt(dot2(scaled * scaled, ones) + KEY_EPS)
    erase = unit * sigmoid(rate)
    row, col = iota((tok_rows, tok_rows), 0), iota((tok_rows, tok_rows), 1)
    running = ((row // CHUNK == col // CHUNK) & (row >= col)).astype(BF16)
    high, low = split(log_decay)
    total = dot(running, high) + dot(running, low)

    strict_rows = iota((CHUNK, PAIR), 0)
    strict_cols = iota((CHUNK, PAIR), 1) % HEAD
    strict = strict_rows > strict_cols
    inclusive = strict_rows >= strict_cols
    eye = (strict_rows == strict_cols).astype(F32)
    same8 = (strict_rows // 8) == (strict_cols // 8)
    lane_first = first_head(CHUNK)

    units = []
    for c in range(chunks):
        rows = slice(c * CHUNK, (c + 1) * CHUNK)
        cum = total[rows]
        last = cum[CHUNK - 1 : CHUNK]
        half = 0.5 * last
        grow = jnp.exp(half - cum)
        shrink = jnp.exp(cum - half)
        half_decay = jnp.exp(half)
        query_unit = unit[rows] * jnp.exp(cum - log_decay[rows] - half)
        query_read = receptance[rows] * shrink
        scaled_erase = erase[rows] * grow
        scaled_key = key[rows] * grow
        for p in range(pairs):
            lanes = slice(p * PAIR, (p + 1) * PAIR)
            units.append(
                dict(
                    c=c,
                    p=p,
                    qu=query_unit[:, lanes],
                    qr=query_read[:, lanes],
                    se=scaled_erase[:, lanes],
                    sk=scaled_key[:, lanes],
                    v=value[rows, lanes],
                    half=half_decay[:, lanes],
                )
            )
    for u in units:
        left = jnp.concatenate([u["qu"], u["qr"]], axis=0)
        right = jnp.concatenate([diagonal(u["se"]), diagonal(u["sk"])], axis=0)
        u["gram"] = dot3(left, right, NT)
    for u in units:
        gram = u.pop("gram")
        u["mix"] = jnp.where(strict, gram[:CHUNK, :PAIR], 0.0)
        u["key_mix"] = jnp.where(strict, gram[:CHUNK, PAIR:], 0.0)
        u["read_erase"] = jnp.where(inclusive, gram[CHUNK:, :PAIR], 0.0)
        u["read_key"] = jnp.where(inclusive, gram[CHUNK:, PAIR:], 0.0)
        u["near"] = jnp.where(same8, u["mix"], 0.0)
        u["far"] = jnp.where(same8, 0.0, u["mix"])
    for u in units:
        u["near2"] = dot3(u["near"], diagonal(u["near"]))
        u["value_part"] = dot3(
            jnp.concatenate([u.pop("key_mix"), u.pop("read_key")], axis=0), diagonal(u["v"])
        )
    for u in units:
        powers = dot3(jnp.concatenate([u["near"], u["near2"]], axis=0), diagonal(u["near2"]))
        u["start"] = eye - u.pop("near") + u.pop("near2") - powers[:CHUNK]
        u["near4"] = powers[CHUNK:]
    for u in units:
        u["inv8"] = u["start"] + dot3(u["start"], diagonal(u.pop("near4")))
        u.pop("start")
    for u in units:
        u["step"] = dot3(u["inv8"], diagonal(u.pop("far")))
    for u in units:
        out = dot3(u["step"], beside(diagonal(u["step"]), diagonal(u["inv8"])))
        u["step2"] = out[:, :PAIR]
        u["inv"] = u.pop("inv8") - out[:, PAIR:]
        u.pop("step")
    for u in units:
        out = dot3(u["step2"], beside(diagonal(u["step2"]), diagonal(u["inv"])))
        u["step4"] = out[:, :PAIR]
        u["inv"] = u["inv"] + out[:, PAIR:]
        u.pop("step2")
    for u in units:
        u["inv"] = u["inv"] + dot3(u.pop("step4"), diagonal(u["inv"]))
    for u in units:
        right = beside(diagonal(u["value_part"][:CHUNK]), diagonal(u["qu"] * u["half"]))
        u["removed"] = -dot3(u.pop("inv"), right)
    for u in units:
        kept = jnp.concatenate([u["se"] * u["half"], u["sk"] * u["half"]], axis=0)
        right = jnp.concatenate(
            [u["removed"], beside(u["v"], jnp.zeros_like(u["v"]))], axis=0
        )
        out = dot3(kept.T, right)
        u["base"] = undiagonal(out[:, :PAIR])
        u["trans"] = undiagonal(out[:, PAIR:]) + eye * (u["half"] * u["half"])
    return units


def local_reads(units):
    for u in units:
        removed = u["removed"]
        right = beside(diagonal(removed[:, :PAIR]), diagonal(removed[:, PAIR:]))
        out = dot3(u["read_erase"], right)
        u["local"] = out[:, :PAIR] + u["value_part"][CHUNK:]
        u["carried"] = out[:, PAIR:] + u["qr"] * u["half"]


def layer_kernel(
    tokens_hbm, gain_ref, decay_hbm, key_hbm, rate_hbm, receptance_hbm, value_hbm,
    key_gain_ref, bias_ref, shift_hbm, extra_hbm,
    conv_value_hbm, conv_gate_hbm, gate_hbm, taps_ref, group_gain_ref, group_shift_ref,
    head_gain_ref, conv_out_hbm, mix_out_hbm,
    out_ref,
    tokens, normed, weights, shift, extra, conv_w, gate_w, conv_out_w, mix_out_w,
    totals, peer_total, pair_states, y_slots, z_slots, extended, halo, conv_rows,
    local_rows, carried_rows, gate_gain, conv_full, mix_sent, mix_full, acc,
    sems, load_sems, pair_send, pair_recv, y_send, y_recv, z_send, z_recv, halo_send, halo_recv,
    conv_send, conv_recv, mix_send, mix_recv,
):
    sp, tp = lax.axis_index("sp"), lax.axis_index("tp")
    core = lax.rem(sp, 2)
    y = lax.rem(sp // 2, 4)
    z = sp // 8
    sibling = sp + 1 - 2 * core
    after, before = lax.rem(sp + 1, 32), lax.rem(sp + 31, 32)
    is_first = core == 0

    def y_of(step):
        return lax.rem(y + step, 4)

    def z_of(step):
        return lax.rem(z + step, 4)

    def x_of(step):
        return lax.rem(tp + step, 4)

    def y_peer(step):
        return (z * 8 + y_of(step) * 2 + core, tp)

    def z_peer(step):
        return (z_of(step) * 8 + y * 2 + core, tp)

    def x_peer(step):
        return (sp, x_of(step))

    def remote(source, target, send, recv, peer):
        return pltpu.make_async_remote_copy(
            src_ref=source, dst_ref=target, send_sem=send, recv_sem=recv,
            device_id=peer, device_id_type=MESH,
        )

    order = (decay_hbm, key_hbm, rate_hbm, receptance_hbm, value_hbm)
    copies = [pltpu.make_async_copy(tokens_hbm, tokens, sems.at[0])]
    for i, source in enumerate(order):
        copies.append(pltpu.make_async_copy(source, weights.at[i], sems.at[1 + i]))
    copies.append(pltpu.make_async_copy(shift_hbm, shift, sems.at[6]))
    copies.append(pltpu.make_async_copy(extra_hbm, extra, sems.at[7]))
    for copy in copies:
        copy.start()

    barrier = pltpu.get_barrier_semaphore()
    peers = [(sibling, tp), (after, tp), (before, tp)]
    for step in (1, 2, 3):
        peers += [y_peer(step), z_peer(step), x_peer(step)]
    for peer in peers:
        pl.semaphore_signal(barrier, inc=1, device_id=peer, device_id_type=MESH)

    loads = [
        pltpu.make_async_copy(conv_value_hbm, conv_w.at[0], load_sems.at[0]),
        pltpu.make_async_copy(conv_gate_hbm, conv_w.at[1], load_sems.at[1]),
        pltpu.make_async_copy(gate_hbm, gate_w, load_sems.at[2]),
        pltpu.make_async_copy(conv_out_hbm, conv_out_w, load_sems.at[3]),
        pltpu.make_async_copy(mix_out_hbm, mix_out_w, load_sems.at[4]),
    ]
    with jax.named_scope("wait_tokens"):
        copies[0].wait()
    with jax.named_scope("norm"):
        normed[...] = normalize(tokens[...], gain_ref[...])
    with jax.named_scope("project"):
        found = []
        for i in range(5):
            copies[1 + i].wait()
            found.append(rounded(dot(normed[...], weights[i])))
        decay, key, rate, receptance, value = found
        copies[6].wait()
        copies[7].wait()
    for load in loads:
        load.start()
    with jax.named_scope("algebra"):
        units = chunk_algebra(
            receptance, key, value, decay, rate, key_gain_ref[...], bias_ref[...], shift[...],
            extra[...],
        )
    with jax.named_scope("totals"):
        prefixes = []
        for p in range(2):
            steps = [(u["trans"], u["base"]) for u in units if u["p"] == p]
            two = compose(steps[1], steps[0], dot3)
            upper = compose(steps[3], steps[2], dot3)
            totals[p] = beside(*compose(upper, two, dot3))
            prefixes.append((steps[0], two, steps[2]))
    with jax.named_scope("barrier"):
        pl.semaphore_wait(barrier, len(peers))
    pair_copy = remote(
        totals.at[1 - core], peer_total, pair_send.at[0], pair_recv.at[0], (sibling, tp)
    )
    pair_copy.start()

    with jax.named_scope("conv_project"):
        loads[0].wait()
        conv_value = rounded(dot(normed[...], conv_w[0]))
        loads[1].wait()
        conv_gate = rounded(dot(normed[...], conv_w[1]))
        conv_input = (conv_value * sigmoid(conv_gate)).astype(BF16)
        conv_rows[...] = conv_input[224:]
        halo_copy = remote(conv_rows, halo, halo_send.at[0], halo_recv.at[0], (after, tp))
        halo_copy.start()
        extended[32:, :] = conv_input.astype(F32)

    with jax.named_scope("pair_wait"):
        pair_copy.wait()
    with jax.named_scope("pair_compose"):
        own, other = totals[core], peer_total[...]
        first = jnp.where(is_first, own, other)
        second = jnp.where(is_first, other, own)
        chip_first = (first[:, :PAIR], first[:, PAIR:])
        chip = compose((second[:, :PAIR], second[:, PAIR:]), chip_first, dot3)
        y_slots[y] = beside(*chip).astype(BF16)
    y_copies = []
    for step in (2, 1, 3):
        copy = remote(
            y_slots.at[y], y_slots.at[y], y_send.at[step - 1], y_recv.at[step - 1], y_peer(step)
        )
        copy.start()
        y_copies.append(copy)

    with jax.named_scope("gate_project"):
        loads[2].wait()
        gated = sigmoid(rounded(dot(normed[...], gate_w[...]))) * head_gain_ref[...]
        gate_gain[0] = gated[:, :PAIR]
        gate_gain[1] = gated[:, PAIR:]
    with jax.named_scope("local_reads"):
        local_reads(units)
        for p in range(2):
            one, two, third = prefixes[p]
            earlier = (None, one, two, compose(third, two, dot3))
            for u in units:
                if u["p"] != p:
                    continue
                c = u["c"]
                rows = slice(c * CHUNK, (c + 1) * CHUNK)
                if c == 0:
                    local_rows[p, rows] = u["local"]
                    carried_rows[p, rows] = u["carried"]
                    continue
                right = beside(diagonal(earlier[c][0]), diagonal(earlier[c][1]))
                out = dot3(u["carried"], right)
                carried_rows[p, rows] = out[:, :PAIR]
                local_rows[p, rows] = out[:, PAIR:] + u["local"]

    with jax.named_scope("y_wait"):
        for copy in y_copies:
            copy.wait_send()
        for step in (1, 3, 2):
            arrived = y_of(4 - step)
            remote(
                y_slots.at[arrived], y_slots.at[arrived], y_send.at[step - 1],
                y_recv.at[step - 1], y_peer(step),
            ).wait_recv()

    def slot(ref, k):
        both = ref[k].astype(F32)
        return both[:, :PAIR], both[:, PAIR:]

    with jax.named_scope("y_compose"):
        c0, c1, c2, c3 = (slot(y_slots, k) for k in range(4))
        c01, c23 = compose(c1, c0, dot1), compose(c3, c2, dot1)
        plane = compose(c23, c01, dot3)
        z_slots[z] = beside(*plane).astype(BF16)
    z_copies = []
    for step in (2, 1, 3):
        copy = remote(
            z_slots.at[z], z_slots.at[z], z_send.at[step - 1], z_recv.at[step - 1], z_peer(step)
        )
        copy.start()
        z_copies.append(copy)
    eye = (iota((HEAD, PAIR), 0) == iota((HEAD, PAIR), 1) % HEAD).astype(F32)
    nothing = jnp.zeros((HEAD, PAIR), F32)

    def pick(index, a, b, c, d):
        return jnp.where(index == 0, a, jnp.where(index == 1, b, jnp.where(index == 2, c, d)))

    with jax.named_scope("before_chip"):
        c012 = compose(c2, c01, dot3)
        before_chip = (
            pick(y, eye, c0[0], c01[0], c012[0]), pick(y, nothing, c0[1], c01[1], c012[1])
        )
        before_second = compose(chip_first, before_chip, dot3)
        trans_both = jnp.concatenate([before_chip[0], before_second[0]], axis=0)
        base_both = jnp.concatenate([before_chip[1], before_second[1]], axis=0)

    with jax.named_scope("halo_wait"):
        halo_copy.wait()
    with jax.named_scope("convolution"):
        extended[:32, :] = jnp.where(sp == 0, 0.0, halo[...].astype(F32))
        taps = taps_ref[...]
        conv_sum = jnp.zeros((256, PAIR), F32)
        for j in range(31):
            conv_sum = conv_sum + taps[j : j + 1] * extended[pl.ds(2 + j, 256), :]
        normal = group_norm(conv_sum, group_ones(PAIR), GROUP_EPS)
        affine = normal * group_gain_ref[...] + group_shift_ref[...]
        conv_out = (affine * sigmoid(affine)).astype(BF16)
        for k in range(4):
            conv_full[0, k] = conv_out[k * 64 : (k + 1) * 64]
    conv_copies = []
    for step in (2, 1, 3):
        copy = remote(
            conv_full.at[0, x_of(step)], conv_full.at[1, tp],
            conv_send.at[step - 1], conv_recv.at[step - 1], x_peer(step),
        )
        copy.start()
        conv_copies.append(copy)

    with jax.named_scope("z_wait"):
        for copy in z_copies:
            copy.wait_send()
        for step in (1, 3, 2):
            arrived = z_of(4 - step)
            remote(
                z_slots.at[arrived], z_slots.at[arrived], z_send.at[step - 1],
                z_recv.at[step - 1], z_peer(step),
            ).wait_recv()
    with jax.named_scope("z_compose"):
        p0, p1, p2 = (slot(z_slots, k) for k in range(3))
        into2 = dot1(p1[0], diagonal(p0[1])) + p1[1]
        last_trans = pick(z, eye, eye, p1[0], p2[0])
        last_base = pick(z, nothing, nothing, p1[1], p2[1])
        inner = pick(z, nothing, p0[1], p0[1], into2)
        out = dot3(trans_both, beside(diagonal(last_trans), diagonal(last_base)))
        states = dot3(out[:, :PAIR], diagonal(inner)) + (out[:, PAIR:] + base_both)
        state_first, state_second = states[:HEAD], states[HEAD:]
        mine = jnp.where(is_first, state_first, state_second)
        pair_states[0] = jnp.where(is_first, state_second, state_first)
    state_copy = remote(
        pair_states.at[0], pair_states.at[1], pair_send.at[1], pair_recv.at[1], (sibling, tp)
    )
    state_copy.start()

    ones = group_ones(PAIR)

    def read_pair(p, state, half):
        readout = local_rows[p] + dot3(carried_rows[p], diagonal(state))
        mix_out = (group_norm(readout, ones, HEAD_EPS) * gate_gain[p]).astype(BF16)
        started = []
        for k in range(4):
            mix_sent[half, k] = mix_out[k * 64 : (k + 1) * 64]
        for step in (2, 1, 3):
            copy = remote(
                mix_sent.at[half, x_of(step)], mix_full.at[half, tp],
                mix_send.at[half, step - 1], mix_recv.at[half, step - 1], x_peer(step),
            )
            copy.start()
            started.append(copy)
        return started

    def out_rows(owner, p):
        return pl.ds(pl.multiple_of(owner * 256 + p * PAIR, PAIR), PAIR)

    with jax.named_scope("read_own"):
        started = read_pair(core, mine, 0)

    with jax.named_scope("conv_project_out"):
        loads[3].wait()
        acc[...] = dot(conv_full[0, tp], conv_out_w[pl.ds(pl.multiple_of(tp * PAIR, PAIR), PAIR), :])
        for copy in conv_copies:
            copy.wait_send()
        for step in (1, 3, 2):
            arrived = x_of(4 - step)
            remote(
                conv_full.at[0, arrived], conv_full.at[1, arrived],
                conv_send.at[step - 1], conv_recv.at[step - 1], x_peer(step),
            ).wait_recv()
            rows = pl.ds(pl.multiple_of(arrived * PAIR, PAIR), PAIR)
            acc[...] += dot(conv_full[1, arrived], conv_out_w[rows, :])
    with jax.named_scope("state_wait"):
        state_copy.wait()
    with jax.named_scope("read_other"):
        started += read_pair(1 - core, pair_states[1], 1)
    with jax.named_scope("mix_own"):
        loads[4].wait()
        acc[...] += dot(mix_sent[0, tp], mix_out_w[out_rows(tp, core), :]) + dot(
            mix_sent[1, tp], mix_out_w[out_rows(tp, 1 - core), :]
        )
        for copy in started:
            copy.wait_send()
    for half in (0, 1):
        for step in (1, 3, 2):
            arrived = x_of(4 - step)
            with jax.named_scope("mix_wait"):
                remote(
                    mix_sent.at[half, arrived], mix_full.at[half, arrived],
                    mix_send.at[half, step - 1], mix_recv.at[half, step - 1], x_peer(step),
                ).wait_recv()
            with jax.named_scope("mix_project"):
                p = core if half == 0 else 1 - core
                acc[...] += dot(mix_full[half, arrived], mix_out_w[out_rows(arrived, p), :])
    out_ref[...] = acc[...].astype(BF16)


VMEM = pl.BlockSpec(memory_space=pltpu.VMEM)
ANY = pl.BlockSpec(memory_space=pltpu.HBM)


def local(
    tokens, input_norm_gain, convolution_value_weight, convolution_gate_weight,
    depthwise_taps_weight, convolution_group_gain, convolution_group_shift, receptance_weight,
    key_weight, value_weight, decay_weight, correction_rate_weight, output_gate_weight,
    key_prenorm_gain, decay_offset_bias, position_decay_shift, extra_log_decay, head_norm_gain,
    convolution_output_weight, attention_output_weight,
):
    dma = pltpu.SemaphoreType.DMA
    return pl.pallas_call(
        layer_kernel,
        name="layer",
        out_shape=jax.ShapeDtypeStruct((64, 2048), BF16),
        in_specs=[ANY, VMEM] + [ANY] * 5 + [VMEM, VMEM] + [ANY] * 5 + [VMEM] * 4 + [ANY] * 2,
        out_specs=VMEM,
        scratch_shapes=[
            pltpu.VMEM((256, 2048), BF16),
            pltpu.VMEM((256, 2048), BF16),
            pltpu.VMEM((5, 2048, 256), BF16),
            pltpu.VMEM((256, 256), F32),
            pltpu.VMEM((256, 256), F32),
            pltpu.VMEM((2, 2048, 128), BF16),
            pltpu.VMEM((2048, 256), BF16),
            pltpu.VMEM((512, 2048), BF16),
            pltpu.VMEM((1024, 2048), BF16),
            pltpu.VMEM((2, 64, 256), F32),
            pltpu.VMEM((64, 256), F32),
            pltpu.VMEM((2, 64, 128), F32),
            pltpu.VMEM((4, 64, 256), BF16),
            pltpu.VMEM((4, 64, 256), BF16),
            pltpu.VMEM((288, 128), F32),
            pltpu.VMEM((32, 128), BF16),
            pltpu.VMEM((32, 128), BF16),
            pltpu.VMEM((2, 256, 128), F32),
            pltpu.VMEM((2, 256, 128), F32),
            pltpu.VMEM((2, 256, 128), F32),
            pltpu.VMEM((2, 4, 64, 128), BF16),
            pltpu.VMEM((2, 4, 64, 128), BF16),
            pltpu.VMEM((2, 4, 64, 128), BF16),
            pltpu.VMEM((64, 2048), F32),
            dma((8,)), dma((5,)), dma((2,)), dma((2,)), dma((3,)), dma((3,)), dma((3,)), dma((3,)),
            dma((1,)), dma((1,)), dma((3,)), dma((3,)), dma((2, 3)), dma((2, 3)),
        ],
        compiler_params=pltpu.CompilerParams(
            collective_id=0, has_side_effects=True, vmem_limit_bytes=66650000
        ),
    )(
        tokens, input_norm_gain.reshape(1, -1), decay_weight, key_weight, correction_rate_weight,
        receptance_weight, value_weight, key_prenorm_gain.reshape(1, -1),
        decay_offset_bias.reshape(1, -1), position_decay_shift, extra_log_decay,
        convolution_value_weight, convolution_gate_weight, output_gate_weight,
        depthwise_taps_weight, convolution_group_gain.reshape(1, -1),
        convolution_group_shift.reshape(1, -1), head_norm_gain.reshape(1, -1),
        convolution_output_weight, attention_output_weight,
    )


def solution(mesh):
    rows, chans, vec = P("sp", None), P(None, "tp"), P("tp")
    placed = (
        rows, P(), chans, chans, chans, vec, vec, chans, chans, chans, chans, chans, chans,
        vec, vec, P("sp", "tp"), P("sp", "tp"), vec, P(), P(),
    )
    return jax.shard_map(
        local, mesh=mesh, in_specs=placed, out_specs=P(("sp", "tp"), None), check_vma=False
    )
```

time: 38.9 us -> 33.1 us (0.85)
  Pallas kernels: 37 us -> 31.3 us
    pallas_call x2 -> x1, Pallas kernels: 37 us -> 31.3 us  [local(): pl.pallas_call(layer_kernel, name='layer', out_shape=jax.ShapeDtypeStruct...]
where the time goes in v2:
time: 33.1 us; the launch traced here: 32.9 us
  Pallas kernels  31.3 us (95%)
  local copies, waits for them, and re-layouts  1.67 us (5%)
    pallas_call x1, Pallas kernels, local(): pl.pallas_call(layer_kernel, name='layer', out_shape=jax.ShapeDtypeStruct...  31.3 us
    unnamed x1, local copies, waits for them, and re-layouts  1.67 us

profile of v2, /device:TPU:1, one launch (start us, length us, event | category | flops | bytes accessed | tf_op | source)
XLA Modules:
  0.0 32.9 jit_solution(7649109596717843175)
XLA Ops:
  0.0 31.3 %layer.1 = bf16[64,2048]{1,0:T(8,128)(2,1)} custom-call(bf16[256,2048]{1,0:T(8,128)(2,1)} %tokens_hbm.1, f32[1,2048]{1,0:T(1,128)} %bitcast.6, bf16[2048,256]{1,0:T(8,128)(2,1)} %decay_hbm.1, bf16[2048,256]{1,0:T(8,128)(2,1)} %key_hbm.1, bf16[2048,256]{1,0:T(8,128)(2,1)} %rate_hbm.1, bf16[2048,256]{1,0:T(8,128)(2,1)} %receptance_hbm.1, ...), custom_call_target="tpu_custom_call" | custom-call | tf_op jit(solution)/shard_map/layer/pallas_call | solution.py:526
  31.3 1.7 %copy.22 = bf16[64,2048]{1,0:T(8,128)(2,1)} copy(bf16[64,2048]{1,0:T(8,128)(2,1)} %layer.1) | data formatting | bytes 524288

commit v3 on v2

--- a/solution.py
+++ b/solution.py
@@ -151,7 +151,7 @@
     for u in units:
         left = jnp.concatenate([u["qu"], u["qr"]], axis=0)
         right = jnp.concatenate([diagonal(u["se"]), diagonal(u["sk"])], axis=0)
-        u["gram"] = dot3(left, right, NT)
+        u["gram"] = dot1(left, right, NT)
     for u in units:
         gram = u.pop("gram")
         u["mix"] = jnp.where(strict, gram[:CHUNK, :PAIR], 0.0)
@@ -162,7 +162,7 @@
         u["far"] = jnp.where(same8, 0.0, u["mix"])
     for u in units:
         u["near2"] = dot3(u["near"], diagonal(u["near"]))
-        u["value_part"] = dot3(
+        u["value_part"] = dot1(
             jnp.concatenate([u.pop("key_mix"), u.pop("read_key")], axis=0), diagonal(u["v"])
         )
     for u in units:
@@ -188,13 +188,13 @@
         u["inv"] = u["inv"] + dot3(u.pop("step4"), diagonal(u["inv"]))
     for u in units:
         right = beside(diagonal(u["value_part"][:CHUNK]), diagonal(u["qu"] * u["half"]))
-        u["removed"] = -dot3(u.pop("inv"), right)
+        u["removed"] = -dot1(u.pop("inv"), right)
     for u in units:
         kept = jnp.concatenate([u["se"] * u["half"], u["sk"] * u["half"]], axis=0)
         right = jnp.concatenate(
             [u["removed"], beside(u["v"], jnp.zeros_like(u["v"]))], axis=0
         )
-        out = dot3(kept.T, right)
+        out = dot1(kept.T, right)
         u["base"] = undiagonal(out[:, :PAIR])
         u["trans"] = undiagonal(out[:, PAIR:]) + eye * (u["half"] * u["half"])
     return units
@@ -204,22 +204,23 @@
     for u in units:
         removed = u["removed"]
         right = beside(diagonal(removed[:, :PAIR]), diagonal(removed[:, PAIR:]))
-        out = dot3(u["read_erase"], right)
+        out = dot1(u["read_erase"], right)
         u["local"] = out[:, :PAIR] + u["value_part"][CHUNK:]
         u["carried"] = out[:, PAIR:] + u["qr"] * u["half"]
 
 
 def layer_kernel(
-    tokens_hbm, gain_ref, decay_hbm, key_hbm, rate_hbm, receptance_hbm, value_hbm,
-    key_gain_ref, bias_ref, shift_hbm, extra_hbm,
-    conv_value_hbm, conv_gate_hbm, gate_hbm, taps_ref, group_gain_ref, group_shift_ref,
-    head_gain_ref, conv_out_hbm, mix_out_hbm,
+    tokens_hbm, gain_hbm, decay_hbm, key_hbm, rate_hbm, receptance_hbm, value_hbm,
+    key_gain_hbm, bias_hbm, shift_hbm, extra_hbm,
+    conv_value_hbm, conv_gate_hbm, gate_hbm, taps_hbm, group_gain_hbm, group_shift_hbm,
+    head_gain_hbm, conv_out_hbm, mix_out_hbm,
     out_ref,
-    tokens, normed, weights, shift, extra, conv_w, gate_w, conv_out_w, mix_out_w,
-    totals, peer_total, pair_states, y_slots, z_slots, extended, halo, conv_rows,
+    gain_ref, key_gain_ref, bias_ref, taps_ref, group_gain_ref, group_shift_ref, head_gain_ref,
+    tokens, normed, weights, shift, extra, gate_w, conv_out_w, mix_out_w,
+    totals, peer_total, pair_states, y_slots, z_slots, y_seen, z_seen, extended, halo, conv_rows,
     local_rows, carried_rows, gate_gain, conv_full, mix_sent, mix_full, acc,
     sems, load_sems, pair_send, pair_recv, y_send, y_recv, z_send, z_recv, halo_send, halo_recv,
-    conv_send, conv_recv, mix_send, mix_recv,
+    conv_send, conv_recv, mix_send, mix_recv, small_sems,
 ):
     sp, tp = lax.axis_index("sp"), lax.axis_index("tp")
     core = lax.rem(sp, 2)
@@ -257,9 +258,33 @@
     copies = [pltpu.make_async_copy(tokens_hbm, tokens, sems.at[0])]
     for i, source in enumerate(order):
         copies.append(pltpu.make_async_copy(source, weights.at[i], sems.at[1 + i]))
-    copies.append(pltpu.make_async_copy(shift_hbm, shift, sems.at[6]))
-    copies.append(pltpu.make_async_copy(extra_hbm, extra, sems.at[7]))
-    for copy in copies:
+    copies.append(
+        pltpu.make_async_copy(conv_value_hbm, weights.at[5, :, pl.ds(0, PAIR)], sems.at[6])
+    )
+    late = [
+        pltpu.make_async_copy(conv_gate_hbm, weights.at[5, :, pl.ds(PAIR, PAIR)], sems.at[7]),
+        pltpu.make_async_copy(shift_hbm, shift, sems.at[8]),
+        pltpu.make_async_copy(extra_hbm, extra, sems.at[9]),
+    ]
+    smalls = [
+        pltpu.make_async_copy(source, target, small_sems.at[i])
+        for i, (source, target) in enumerate(
+            (
+                (gain_hbm, gain_ref),
+                (key_gain_hbm, key_gain_ref),
+                (bias_hbm, bias_ref),
+                (taps_hbm, taps_ref),
+                (group_gain_hbm, group_gain_ref),
+                (group_shift_hbm, group_shift_ref),
+                (head_gain_hbm, head_gain_ref),
+            )
+        )
+    ]
+    copies[0].start()
+    smalls[0].start()
+    for copy in copies[1:] + late:
+        copy.start()
+    for copy in smalls[1:]:
         copy.start()
 
     barrier = pltpu.get_barrier_semaphore()
@@ -270,24 +295,34 @@
         pl.semaphore_signal(barrier, inc=1, device_id=peer, device_id_type=MESH)
 
     loads = [
-        pltpu.make_async_copy(conv_value_hbm, conv_w.at[0], load_sems.at[0]),
-        pltpu.make_async_copy(conv_gate_hbm, conv_w.at[1], load_sems.at[1]),
-        pltpu.make_async_copy(gate_hbm, gate_w, load_sems.at[2]),
-        pltpu.make_async_copy(conv_out_hbm, conv_out_w, load_sems.at[3]),
-        pltpu.make_async_copy(mix_out_hbm, mix_out_w, load_sems.at[4]),
+        pltpu.make_async_copy(gate_hbm, gate_w, load_sems.at[0]),
+        pltpu.make_async_copy(conv_out_hbm, conv_out_w, load_sems.at[1]),
+        pltpu.make_async_copy(mix_out_hbm, mix_out_w, load_sems.at[2]),
     ]
+    eye = (iota((HEAD, 2 * PAIR), 0) == iota((HEAD, 2 * PAIR), 1) % HEAD) & (
+        iota((HEAD, 2 * PAIR), 1) < PAIR
+    )
+    identity = jnp.where(eye, 1.0, 0.0).astype(BF16)
+    for k in range(3):
+        y_seen[k] = identity
+        z_seen[k] = identity
     with jax.named_scope("wait_tokens"):
         copies[0].wait()
+        smalls[0].wait()
     with jax.named_scope("norm"):
         normed[...] = normalize(tokens[...], gain_ref[...])
     with jax.named_scope("project"):
         found = []
-        for i in range(5):
+        for i in (0, 2, 4):
             copies[1 + i].wait()
-            found.append(rounded(dot(normed[...], weights[i])))
-        decay, key, rate, receptance, value = found
-        copies[6].wait()
-        copies[7].wait()
+            copies[2 + i].wait()
+            if i == 4:
+                late[0].wait()
+            found.append(dot(normed[...], weights[i]))
+            found.append(dot(normed[...], weights[i + 1]))
+        decay, key, rate, receptance, value, conv_both = (rounded(rows) for rows in found)
+        for copy in late[1:] + smalls[1:]:
+            copy.wait()
     for load in loads:
         load.start()
     with jax.named_scope("algebra"):
@@ -311,14 +346,11 @@
     pair_copy.start()
 
     with jax.named_scope("conv_project"):
-        loads[0].wait()
-        conv_value = rounded(dot(normed[...], conv_w[0]))
-        loads[1].wait()
-        conv_gate = rounded(dot(normed[...], conv_w[1]))
-        conv_input = (conv_value * sigmoid(conv_gate)).astype(BF16)
+        conv_input = (conv_both[:, :PAIR] * sigmoid(conv_both[:, PAIR:])).astype(BF16)
         conv_rows[...] = conv_input[224:]
         halo_copy = remote(conv_rows, halo, halo_send.at[0], halo_recv.at[0], (after, tp))
-        halo_copy.start()
+        pl.when(sp < 31)(halo_copy.start)
+        extended[:32, :] = jnp.zeros((32, PAIR), F32)
         extended[32:, :] = conv_input.astype(F32)
 
     with jax.named_scope("pair_wait"):
@@ -339,7 +371,7 @@
         y_copies.append(copy)
 
     with jax.named_scope("gate_project"):
-        loads[2].wait()
+        loads[0].wait()
         gated = sigmoid(rounded(dot(normed[...], gate_w[...]))) * head_gain_ref[...]
         gate_gain[0] = gated[:, :PAIR]
         gate_gain[1] = gated[:, PAIR:]
@@ -347,7 +379,7 @@
         local_reads(units)
         for p in range(2):
             one, two, third = prefixes[p]
-            earlier = (None, one, two, compose(third, two, dot3))
+            earlier = (None, one, two, compose(third, two, dot1))
             for u in units:
                 if u["p"] != p:
                     continue
@@ -358,55 +390,45 @@
                     carried_rows[p, rows] = u["carried"]
                     continue
                 right = beside(diagonal(earlier[c][0]), diagonal(earlier[c][1]))
-                out = dot3(u["carried"], right)
+                out = dot1(u["carried"], right)
                 carried_rows[p, rows] = out[:, :PAIR]
                 local_rows[p, rows] = out[:, PAIR:] + u["local"]
 
-    with jax.named_scope("y_wait"):
-        for copy in y_copies:
-            copy.wait_send()
-        for step in (1, 3, 2):
-            arrived = y_of(4 - step)
-            remote(
-                y_slots.at[arrived], y_slots.at[arrived], y_send.at[step - 1],
-                y_recv.at[step - 1], y_peer(step),
-            ).wait_recv()
+    def y_arrival(step):
+        arrived = y_of(4 - step)
+        return remote(
+            y_slots.at[arrived], y_slots.at[arrived], y_send.at[step - 1], y_recv.at[step - 1],
+            y_peer(step),
+        )
+
+    with jax.named_scope("y_wait_lower"):
+        for step in (1, 2, 3):
+
+            @pl.when(step <= y)
+            def _(step=step):
+                y_arrival(step).wait_recv()
+                y_seen[y - step] = y_slots[y - step]
 
     def slot(ref, k):
         both = ref[k].astype(F32)
         return both[:, :PAIR], both[:, PAIR:]
 
-    with jax.named_scope("y_compose"):
-        c0, c1, c2, c3 = (slot(y_slots, k) for k in range(4))
-        c01, c23 = compose(c1, c0, dot1), compose(c3, c2, dot1)
-        plane = compose(c23, c01, dot3)
-        z_slots[z] = beside(*plane).astype(BF16)
-    z_copies = []
-    for step in (2, 1, 3):
-        copy = remote(
-            z_slots.at[z], z_slots.at[z], z_send.at[step - 1], z_recv.at[step - 1], z_peer(step)
-        )
-        copy.start()
-        z_copies.append(copy)
-    eye = (iota((HEAD, PAIR), 0) == iota((HEAD, PAIR), 1) % HEAD).astype(F32)
-    nothing = jnp.zeros((HEAD, PAIR), F32)
-
-    def pick(index, a, b, c, d):
-        return jnp.where(index == 0, a, jnp.where(index == 1, b, jnp.where(index == 2, c, d)))
-
     with jax.named_scope("before_chip"):
-        c012 = compose(c2, c01, dot3)
-        before_chip = (
-            pick(y, eye, c0[0], c01[0], c012[0]), pick(y, nothing, c0[1], c01[1], c012[1])
+        before_chip = compose(
+            slot(y_seen, 2), compose(slot(y_seen, 1), slot(y_seen, 0), dot1), dot3
         )
         before_second = compose(chip_first, before_chip, dot3)
         trans_both = jnp.concatenate([before_chip[0], before_second[0]], axis=0)
         base_both = jnp.concatenate([before_chip[1], before_second[1]], axis=0)
 
     with jax.named_scope("halo_wait"):
-        halo_copy.wait()
+
+        @pl.when(sp > 0)
+        def _():
+            halo_copy.wait_recv()
+            extended[:32, :] = halo[...].astype(F32)
+
     with jax.named_scope("convolution"):
-        extended[:32, :] = jnp.where(sp == 0, 0.0, halo[...].astype(F32))
         taps = taps_ref[...]
         conv_sum = jnp.zeros((256, PAIR), F32)
         for j in range(31):
@@ -425,22 +447,42 @@
         copy.start()
         conv_copies.append(copy)
 
+    with jax.named_scope("y_wait_upper"):
+        for step in (1, 2, 3):
+            pl.when(step > y)(y_arrival(step).wait_recv)
+
+    def z_copy(step):
+        return remote(
+            z_slots.at[z], z_slots.at[z], z_send.at[step - 1], z_recv.at[step - 1], z_peer(step)
+        )
+
+    with jax.named_scope("plane"):
+
+        @pl.when(z < 3)
+        def _():
+            lower = compose(slot(y_slots, 1), slot(y_slots, 0), dot1)
+            upper = compose(slot(y_slots, 3), slot(y_slots, 2), dot1)
+            z_slots[z] = beside(*compose(upper, lower, dot3)).astype(BF16)
+            z_copy(1).start()
+            pl.when(z < 2)(z_copy(2).start)
+            pl.when(z < 1)(z_copy(3).start)
+
     with jax.named_scope("z_wait"):
-        for copy in z_copies:
-            copy.wait_send()
         for step in (1, 3, 2):
-            arrived = z_of(4 - step)
-            remote(
-                z_slots.at[arrived], z_slots.at[arrived], z_send.at[step - 1],
-                z_recv.at[step - 1], z_peer(step),
-            ).wait_recv()
+
+            @pl.when(step <= z)
+            def _(step=step):
+                below = z - step
+                remote(
+                    z_slots.at[below], z_slots.at[below], z_send.at[step - 1],
+                    z_recv.at[step - 1], z_peer(step),
+                ).wait_recv()
+                z_seen[below] = z_slots[below]
+
     with jax.named_scope("z_compose"):
-        p0, p1, p2 = (slot(z_slots, k) for k in range(3))
-        into2 = dot1(p1[0], diagonal(p0[1])) + p1[1]
-        last_trans = pick(z, eye, eye, p1[0], p2[0])
-        last_base = pick(z, nothing, nothing, p1[1], p2[1])
-        inner = pick(z, nothing, p0[1], p0[1], into2)
-        out = dot3(trans_both, beside(diagonal(last_trans), diagonal(last_base)))
+        p0, p1, p2 = (slot(z_seen, k) for k in range(3))
+        inner = dot1(p1[0], diagonal(p0[1])) + p1[1]
+        out = dot3(trans_both, beside(diagonal(p2[0]), diagonal(p2[1])))
         states = dot3(out[:, :PAIR], diagonal(inner)) + (out[:, PAIR:] + base_both)
         state_first, state_second = states[:HEAD], states[HEAD:]
         mine = jnp.where(is_first, state_first, state_second)
@@ -474,10 +516,8 @@
         started = read_pair(core, mine, 0)
 
     with jax.named_scope("conv_project_out"):
-        loads[3].wait()
+        loads[1].wait()
         acc[...] = dot(conv_full[0, tp], conv_out_w[pl.ds(pl.multiple_of(tp * PAIR, PAIR), PAIR), :])
-        for copy in conv_copies:
-            copy.wait_send()
         for step in (1, 3, 2):
             arrived = x_of(4 - step)
             remote(
@@ -491,12 +531,10 @@
     with jax.named_scope("read_other"):
         started += read_pair(1 - core, pair_states[1], 1)
     with jax.named_scope("mix_own"):
-        loads[4].wait()
+        loads[2].wait()
         acc[...] += dot(mix_sent[0, tp], mix_out_w[out_rows(tp, core), :]) + dot(
             mix_sent[1, tp], mix_out_w[out_rows(tp, 1 - core), :]
         )
-        for copy in started:
-            copy.wait_send()
     for half in (0, 1):
         for step in (1, 3, 2):
             arrived = x_of(4 - step)
@@ -509,6 +547,11 @@
                 p = core if half == 0 else 1 - core
                 acc[...] += dot(mix_full[half, arrived], mix_out_w[out_rows(arrived, p), :])
     out_ref[...] = acc[...].astype(BF16)
+    for copy in y_copies + conv_copies + started:
+        copy.wait_send()
+    pl.when(sp < 31)(halo_copy.wait_send)
+    for step in (1, 2, 3):
+        pl.when(z + step < 4)(z_copy(step).wait_send)
 
 
 VMEM = pl.BlockSpec(memory_space=pltpu.VMEM)
@@ -526,16 +569,22 @@
     return pl.pallas_call(
         layer_kernel,
         name="layer",
-        out_shape=jax.ShapeDtypeStruct((64, 2048), BF16),
-        in_specs=[ANY, VMEM] + [ANY] * 5 + [VMEM, VMEM] + [ANY] * 5 + [VMEM] * 4 + [ANY] * 2,
+        out_shape=pltpu.VMEM((64, 2048), BF16),
+        in_specs=[ANY] * 20,
         out_specs=VMEM,
         scratch_shapes=[
+            pltpu.VMEM((1, 2048), F32),
+            pltpu.VMEM((1, 256), F32),
+            pltpu.VMEM((1, 256), F32),
+            pltpu.VMEM((31, 128), F32),
+            pltpu.VMEM((1, 128), F32),
+            pltpu.VMEM((1, 128), F32),
+            pltpu.VMEM((1, 256), F32),
             pltpu.VMEM((256, 2048), BF16),
             pltpu.VMEM((256, 2048), BF16),
-            pltpu.VMEM((5, 2048, 256), BF16),
+            pltpu.VMEM((6, 2048, 256), BF16),
             pltpu.VMEM((256, 256), F32),
             pltpu.VMEM((256, 256), F32),
-            pltpu.VMEM((2, 2048, 128), BF16),
             pltpu.VMEM((2048, 256), BF16),
             pltpu.VMEM((512, 2048), BF16),
             pltpu.VMEM((1024, 2048), BF16),
@@ -544,6 +593,8 @@
             pltpu.VMEM((2, 64, 128), F32),
             pltpu.VMEM((4, 64, 256), BF16),
             pltpu.VMEM((4, 64, 256), BF16),
+            pltpu.VMEM((3, 64, 256), BF16),
+            pltpu.VMEM((3, 64, 256), BF16),
             pltpu.VMEM((288, 128), F32),
             pltpu.VMEM((32, 128), BF16),
             pltpu.VMEM((32, 128), BF16),
@@ -554,20 +605,25 @@
             pltpu.VMEM((2, 4, 64, 128), BF16),
             pltpu.VMEM((2, 4, 64, 128), BF16),
             pltpu.VMEM((64, 2048), F32),
-            dma((8,)), dma((5,)), dma((2,)), dma((2,)), dma((3,)), dma((3,)), dma((3,)), dma((3,)),
-            dma((1,)), dma((1,)), dma((3,)), dma((3,)), dma((2, 3)), dma((2, 3)),
+            dma((10,)), dma((3,)), dma((2,)), dma((2,)), dma((3,)), dma((3,)), dma((3,)), dma((3,)),
+            dma((1,)), dma((1,)), dma((3,)), dma((3,)), dma((2, 3)), dma((2, 3)), dma((7,)),
         ],
         compiler_params=pltpu.CompilerParams(
-            collective_id=0, has_side_effects=True, vmem_limit_bytes=66650000
+            collective_id=0, has_side_effects=True, vmem_limit_bytes=56000000
         ),
     )(
-        tokens, input_norm_gain.reshape(1, -1), decay_weight, key_weight, correction_rate_weight,
-        receptance_weight, value_weight, key_prenorm_gain.reshape(1, -1),
-        decay_offset_bias.reshape(1, -1), position_decay_shift, extra_log_decay,
-        convolution_value_weight, convolution_gate_weight, output_gate_weight,
-        depthwise_taps_weight, convolution_group_gain.reshape(1, -1),
-        convolution_group_shift.reshape(1, -1), head_norm_gain.reshape(1, -1),
-        convolution_output_weight, attention_output_weight,
+        *(
+            pltpu.with_memory_space_constraint(operand, pltpu.HBM)
+            for operand in (
+                tokens, input_norm_gain.reshape(1, -1), decay_weight, key_weight,
+                correction_rate_weight, receptance_weight, value_weight,
+                key_prenorm_gain.reshape(1, -1), decay_offset_bias.reshape(1, -1),
+                position_decay_shift, extra_log_decay, convolution_value_weight,
+                convolution_gate_weight, output_gate_weight, depthwise_taps_weight,
+                convolution_group_gain.reshape(1, -1), convolution_group_shift.reshape(1, -1),
+                head_norm_gain.reshape(1, -1), convolution_output_weight, attention_output_weight,
+            )
+        )
     )
 
 

time: 33.1 us -> 25.2 us (0.76)
  the two profiles are of different devices: /device:TPU:1 before, /device:TPU:96 now
where the time goes in v3:
time: 25.2 us; the launch traced here: 25.1 us
  Pallas kernels  24.4 us (97%)
  local copies, waits for them, and re-layouts  0.71 us (3%)
    pallas_call x1, Pallas kernels, local(): pl.pallas_call(layer_kernel, name='layer', out_shape=pltpu.VMEM((64, 2048...  24.4 us
    unnamed x1, local copies, waits for them, and re-layouts  0.71 us

profile of v3, /device:TPU:96, one launch (start us, length us, event | category | flops | bytes accessed | tf_op | source)
XLA Modules:
  0.0 25.1 jit_solution(5313507386848511843)
XLA Ops:
  0.0 24.4 %layer.1 = bf16[64,2048]{1,0:T(8,128)(2,1)S(1)} custom-call(bf16[256,2048]{1,0:T(8,128)(2,1)} %tokens_hbm.1, f32[1,2048]{1,0:T(1,128)} %bitcast.6, bf16[2048,256]{1,0:T(8,128)(2,1)} %decay_hbm.1, bf16[2048,256]{1,0:T(8,128)(2,1)} %key_hbm.1, bf16[2048,256]{1,0:T(8,128)(2,1)} %rate_hbm.1, bf16[2048,256]{1,0:T(8,128)(2,1)} %receptance_hbm.1, ...), custom_call_target="tpu_custom_call" | custom-call | tf_op jit(solution)/shard_map/layer/pallas_call | solution.py:569
  24.4 0.7 %copy.22 = bf16[64,2048]{1,0:T(8,128)(2,1)} copy(bf16[64,2048]{1,0:T(8,128)(2,1)S(1)} %layer.1) | data formatting | bytes 524288

commit v4 on v3

--- a/solution.py
+++ b/solution.py
@@ -108,6 +108,7 @@
     ones = group_ones(width)
     unit = scaled * lax.rsqrt(dot2(scaled * scaled, ones) + KEY_EPS)
     erase = unit * sigmoid(rate)
+    value = value - dot(value.astype(BF16), ones) * (1.0 / HEAD)
     row, col = iota((tok_rows, tok_rows), 0), iota((tok_rows, tok_rows), 1)
     running = ((row // CHUNK == col // CHUNK) & (row >= col)).astype(BF16)
     high, low = split(log_decay)
@@ -173,22 +174,21 @@
         u["inv8"] = u["start"] + dot3(u["start"], diagonal(u.pop("near4")))
         u.pop("start")
     for u in units:
-        u["step"] = dot3(u["inv8"], diagonal(u.pop("far")))
-    for u in units:
-        out = dot3(u["step"], beside(diagonal(u["step"]), diagonal(u["inv8"])))
-        u["step2"] = out[:, :PAIR]
-        u["inv"] = u.pop("inv8") - out[:, PAIR:]
-        u.pop("step")
-    for u in units:
-        out = dot3(u["step2"], beside(diagonal(u["step2"]), diagonal(u["inv"])))
-        u["step4"] = out[:, :PAIR]
-        u["inv"] = u["inv"] + out[:, PAIR:]
-        u.pop("step2")
-    for u in units:
-        u["inv"] = u["inv"] + dot3(u.pop("step4"), diagonal(u["inv"]))
-    for u in units:
-        right = beside(diagonal(u["value_part"][:CHUNK]), diagonal(u["qu"] * u["half"]))
-        u["removed"] = -dot1(u.pop("inv"), right)
+        right = beside(
+            diagonal(u.pop("far")), diagonal(u["value_part"][:CHUNK]), diagonal(u["qu"] * u["half"])
+        )
+        out = dot1(u.pop("inv8"), right)
+        u["step"], u["removed"] = out[:, :PAIR], -out[:, PAIR:]
+    for sign, last in ((-1.0, False), (1.0, False), (1.0, True)):
+        for u in units:
+            step, removed = u.pop("step"), u["removed"]
+            parts = [diagonal(removed[:, :PAIR]), diagonal(removed[:, PAIR:])]
+            if not last:
+                parts.append(diagonal(step))
+            out = dot1(step, beside(*parts))
+            u["removed"] = removed + sign * out[:, : 2 * PAIR]
+            if not last:
+                u["step"] = out[:, 2 * PAIR :]
     for u in units:
         kept = jnp.concatenate([u["se"] * u["half"], u["sk"] * u["half"]], axis=0)
         right = jnp.concatenate(
@@ -217,33 +217,27 @@
     out_ref,
     gain_ref, key_gain_ref, bias_ref, taps_ref, group_gain_ref, group_shift_ref, head_gain_ref,
     tokens, normed, weights, shift, extra, gate_w, conv_out_w, mix_out_w,
-    totals, peer_total, pair_states, y_slots, z_slots, y_seen, z_seen, extended, halo, conv_rows,
+    totals, peer_total, pair_states, y_slots, z_slots, y_seen, z_seen, raw_slots, raw_seen, extended, halo, conv_rows,
     local_rows, carried_rows, gate_gain, conv_full, mix_sent, mix_full, acc,
     sems, load_sems, pair_send, pair_recv, y_send, y_recv, z_send, z_recv, halo_send, halo_recv,
-    conv_send, conv_recv, mix_send, mix_recv, small_sems,
+    conv_send, conv_recv, mix_send, mix_recv, small_sems, raw_send, raw_recv,
 ):
     sp, tp = lax.axis_index("sp"), lax.axis_index("tp")
     core = lax.rem(sp, 2)
     y = lax.rem(sp // 2, 4)
     z = sp // 8
     sibling = sp + 1 - 2 * core
-    after, before = lax.rem(sp + 1, 32), lax.rem(sp + 31, 32)
+    after = lax.rem(sp + 1, 32)
     is_first = core == 0
 
-    def y_of(step):
-        return lax.rem(y + step, 4)
-
-    def z_of(step):
-        return lax.rem(z + step, 4)
+    def y_source(step):
+        return z * 8 + lax.rem(y + 4 - step, 4) * 2 + core
+
+    def y_target(step):
+        return z * 8 + lax.rem(y + step, 4) * 2 + core
 
     def x_of(step):
         return lax.rem(tp + step, 4)
-
-    def y_peer(step):
-        return (z * 8 + y_of(step) * 2 + core, tp)
-
-    def z_peer(step):
-        return (z_of(step) * 8 + y * 2 + core, tp)
 
     def x_peer(step):
         return (sp, x_of(step))
@@ -258,13 +252,9 @@
     copies = [pltpu.make_async_copy(tokens_hbm, tokens, sems.at[0])]
     for i, source in enumerate(order):
         copies.append(pltpu.make_async_copy(source, weights.at[i], sems.at[1 + i]))
-    copies.append(
-        pltpu.make_async_copy(conv_value_hbm, weights.at[5, :, pl.ds(0, PAIR)], sems.at[6])
-    )
     late = [
-        pltpu.make_async_copy(conv_gate_hbm, weights.at[5, :, pl.ds(PAIR, PAIR)], sems.at[7]),
-        pltpu.make_async_copy(shift_hbm, shift, sems.at[8]),
-        pltpu.make_async_copy(extra_hbm, extra, sems.at[9]),
+        pltpu.make_async_copy(shift_hbm, shift, sems.at[6]),
+        pltpu.make_async_copy(extra_hbm, extra, sems.at[7]),
     ]
     smalls = [
         pltpu.make_async_copy(source, target, small_sems.at[i])
@@ -288,14 +278,31 @@
         copy.start()
 
     barrier = pltpu.get_barrier_semaphore()
-    peers = [(sibling, tp), (after, tp), (before, tp)]
+
+    def greet(peer):
+        pl.semaphore_signal(barrier, inc=1, device_id=peer, device_id_type=MESH)
+
+    greet((sibling, tp))
+    pl.when(sp > 0)(lambda: greet((sp - 1, tp)))
     for step in (1, 2, 3):
-        peers += [y_peer(step), z_peer(step), x_peer(step)]
-    for peer in peers:
-        pl.semaphore_signal(barrier, inc=1, device_id=peer, device_id_type=MESH)
+        meets = (step <= y) | ((z < 3) & (y > 0)) if step == 1 else (step <= y) | (z < 3)
+        pl.when(meets)(lambda step=step: greet((y_source(step), tp)))
+        pl.when((y == 0) & (step <= z))(
+            lambda step=step: greet(((z - step) * 8 + 6 + core, tp))
+        )
+        pl.when(step <= z)(lambda step=step: greet((sp - 8 * step, tp)))
+        greet(x_peer(step))
+    targets = (
+        4 + jnp.where(sp < 31, 1, 0) + jnp.where(z < 3, jnp.where(y == 3, 2, 3), 3 - y) + (3 - z)
+        + jnp.where(y == 3, 3 - z, 0)
+    )
 
     loads = [
         pltpu.make_async_copy(gate_hbm, gate_w, load_sems.at[0]),
+        pltpu.make_async_copy(conv_value_hbm, weights.at[5, :, pl.ds(0, PAIR)], load_sems.at[3]),
+        pltpu.make_async_copy(
+            conv_gate_hbm, weights.at[5, :, pl.ds(PAIR, PAIR)], load_sems.at[4]
+        ),
         pltpu.make_async_copy(conv_out_hbm, conv_out_w, load_sems.at[1]),
         pltpu.make_async_copy(mix_out_hbm, mix_out_w, load_sems.at[2]),
     ]
@@ -305,7 +312,9 @@
     identity = jnp.where(eye, 1.0, 0.0).astype(BF16)
     for k in range(3):
         y_seen[k] = identity
-        z_seen[k] = identity
+        raw_seen[k] = identity
+        z_seen[k, 0] = identity[:, :PAIR]
+        z_seen[k, 1] = identity[:, PAIR:]
     with jax.named_scope("wait_tokens"):
         copies[0].wait()
         smalls[0].wait()
@@ -313,15 +322,20 @@
         normed[...] = normalize(tokens[...], gain_ref[...])
     with jax.named_scope("project"):
         found = []
-        for i in (0, 2, 4):
+        for i in (0, 2):
             copies[1 + i].wait()
             copies[2 + i].wait()
-            if i == 4:
-                late[0].wait()
             found.append(dot(normed[...], weights[i]))
             found.append(dot(normed[...], weights[i + 1]))
-        decay, key, rate, receptance, value, conv_both = (rounded(rows) for rows in found)
-        for copy in late[1:] + smalls[1:]:
+        copies[5].wait()
+        half = weights.shape[1] // 2
+        keep = jnp.where(sp < 32, 1.0, 0.0)
+        found.append(
+            dot(normed[:, :half], weights[4, :half, :])
+            + keep * dot(normed[:, half:], weights[4, half:, :])
+        )
+        decay, key, rate, receptance, value = (rounded(rows) for rows in found)
+        for copy in late + smalls[1:]:
             copy.wait()
     for load in loads:
         load.start()
@@ -339,13 +353,17 @@
             totals[p] = beside(*compose(upper, two, dot3))
             prefixes.append((steps[0], two, steps[2]))
     with jax.named_scope("barrier"):
-        pl.semaphore_wait(barrier, len(peers))
+        pl.semaphore_wait(barrier, targets)
     pair_copy = remote(
         totals.at[1 - core], peer_total, pair_send.at[0], pair_recv.at[0], (sibling, tp)
     )
     pair_copy.start()
 
     with jax.named_scope("conv_project"):
+        for load in loads[:3]:
+            load.wait()
+        gate_rows = dot(normed[...], gate_w[...])
+        conv_both = rounded(dot(normed[...], weights[5]))
         conv_input = (conv_both[:, :PAIR] * sigmoid(conv_both[:, PAIR:])).astype(BF16)
         conv_rows[...] = conv_input[224:]
         halo_copy = remote(conv_rows, halo, halo_send.at[0], halo_recv.at[0], (after, tp))
@@ -353,6 +371,10 @@
         extended[:32, :] = jnp.zeros((32, PAIR), F32)
         extended[32:, :] = conv_input.astype(F32)
 
+    with jax.named_scope("gate_project"):
+        gated = sigmoid(rounded(gate_rows)) * head_gain_ref[...]
+        gate_gain[0] = gated[:, :PAIR]
+        gate_gain[1] = gated[:, PAIR:]
     with jax.named_scope("pair_wait"):
         pair_copy.wait()
     with jax.named_scope("pair_compose"):
@@ -362,19 +384,33 @@
         chip_first = (first[:, :PAIR], first[:, PAIR:])
         chip = compose((second[:, :PAIR], second[:, PAIR:]), chip_first, dot3)
         y_slots[y] = beside(*chip).astype(BF16)
-    y_copies = []
-    for step in (2, 1, 3):
-        copy = remote(
-            y_slots.at[y], y_slots.at[y], y_send.at[step - 1], y_recv.at[step - 1], y_peer(step)
-        )
-        copy.start()
-        y_copies.append(copy)
-
-    with jax.named_scope("gate_project"):
-        loads[0].wait()
-        gated = sigmoid(rounded(dot(normed[...], gate_w[...]))) * head_gain_ref[...]
-        gate_gain[0] = gated[:, :PAIR]
-        gate_gain[1] = gated[:, PAIR:]
+
+    def y_copy(step, slot, peer):
+        return remote(
+            y_slots.at[slot], y_slots.at[slot], y_send.at[step - 1], y_recv.at[step - 1],
+            (peer, tp),
+        )
+
+    def raw_copy(up, slot, plane, peer):
+        return remote(
+            y_slots.at[slot], raw_slots.at[plane], raw_send.at[up - 1], raw_recv.at[plane],
+            (peer, tp),
+        )
+
+    def raw_target(up):
+        return (z + up) * 8 + core
+
+    for up in (1, 2, 3):
+        pl.when((y == 3) & (z + up < 4))(
+            lambda up=up: raw_copy(up, y, z, raw_target(up)).start()
+        )
+
+    def y_sends(step):
+        return (y + step < 4) | ((z < 3) & (y < 3)) if step == 1 else (y + step < 4) | (z < 3)
+
+    for step in (2, 3, 1):
+        pl.when(y_sends(step))(lambda step=step: y_copy(step, y, y_target(step)).start())
+
     with jax.named_scope("local_reads"):
         local_reads(units)
         for p in range(2):
@@ -394,19 +430,12 @@
                 carried_rows[p, rows] = out[:, :PAIR]
                 local_rows[p, rows] = out[:, PAIR:] + u["local"]
 
-    def y_arrival(step):
-        arrived = y_of(4 - step)
-        return remote(
-            y_slots.at[arrived], y_slots.at[arrived], y_send.at[step - 1], y_recv.at[step - 1],
-            y_peer(step),
-        )
-
     with jax.named_scope("y_wait_lower"):
         for step in (1, 2, 3):
 
             @pl.when(step <= y)
             def _(step=step):
-                y_arrival(step).wait_recv()
+                y_copy(step, y - step, sibling).wait_recv()
                 y_seen[y - step] = y_slots[y - step]
 
     def slot(ref, k):
@@ -447,43 +476,97 @@
         copy.start()
         conv_copies.append(copy)
 
-    with jax.named_scope("y_wait_upper"):
-        for step in (1, 2, 3):
-            pl.when(step > y)(y_arrival(step).wait_recv)
-
-    def z_copy(step):
+    def z_copy(up, kind, slot, peer):
         return remote(
-            z_slots.at[z], z_slots.at[z], z_send.at[step - 1], z_recv.at[step - 1], z_peer(step)
-        )
+            z_slots.at[slot, kind], z_slots.at[slot, kind], z_send.at[up - 1, kind],
+            z_recv.at[slot, kind], (peer, tp),
+        )
+
+    def z_column(up):
+        z_copy(up, 1, z, sp + 8 * up).start()
+        pl.when(z > 0)(z_copy(up, 0, z, sp + 8 * up).start)
+
+    def upper(step):
+        y_copy(step, lax.rem(y + 4 - step, 4), sibling).wait_recv()
 
     with jax.named_scope("plane"):
 
         @pl.when(z < 3)
         def _():
+            for step in (3, 2):
+                pl.when(step > y)(lambda step=step: upper(step))
             lower = compose(slot(y_slots, 1), slot(y_slots, 0), dot1)
-            upper = compose(slot(y_slots, 3), slot(y_slots, 2), dot1)
-            z_slots[z] = beside(*compose(upper, lower, dot3)).astype(BF16)
-            z_copy(1).start()
-            pl.when(z < 2)(z_copy(2).start)
-            pl.when(z < 1)(z_copy(3).start)
+
+            def store(total):
+                z_slots[z, 0] = total[0].astype(BF16)
+                z_slots[z, 1] = total[1].astype(BF16)
+
+            @pl.when(y == 0)
+            def _():
+                store(compose(slot(y_slots, 2), lower, dot3))
+
+            @pl.when(y > 0)
+            def _():
+                store(compose(compose(slot(y_slots, 3), slot(y_slots, 2), dot1), lower, dot3))
+
+            z_column(1)
+            pl.when(z < 2)(lambda: z_column(2))
+            pl.when(z < 1)(lambda: z_column(3))
+
+    def z_arrival(below):
+        @pl.when(below > 0)
+        def _():
+            z_copy(1, 0, below, sibling).wait_recv()
+
+        z_copy(1, 1, below, sibling).wait_recv()
 
     with jax.named_scope("z_wait"):
-        for step in (1, 3, 2):
-
-            @pl.when(step <= z)
-            def _(step=step):
-                below = z - step
-                remote(
-                    z_slots.at[below], z_slots.at[below], z_send.at[step - 1],
-                    z_recv.at[step - 1], z_peer(step),
-                ).wait_recv()
-                z_seen[below] = z_slots[below]
+        for below in range(2):
+
+            @pl.when(below < z - 1)
+            def _(below=below):
+                z_arrival(below)
+                if below > 0:
+                    z_seen[below, 0] = z_slots[below, 0]
+                z_seen[below, 1] = z_slots[below, 1]
+
+        for below in range(3):
+
+            @pl.when((y == 0) & (below < z))
+            def _(below=below):
+                raw_copy(1, 0, below, sibling).wait_recv()
+                raw_seen[jnp.where(below < z - 1, below, 2)] = raw_slots[below]
+
+        def through(parts, state):
+            return dot3(parts[0], diagonal(state)) + parts[1]
+
+        def plane_below(k):
+            return z_seen[k, 0].astype(F32), z_seen[k, 1].astype(F32)
+
+        far = through(slot(raw_seen, 0), z_seen[0, 1].astype(F32))
+        far = through(slot(raw_seen, 1), through(plane_below(1), far))
+        passed = raw_seen[2]
+        out = dot3(
+            trans_both,
+            beside(
+                diagonal(passed[:, :PAIR].astype(F32)), diagonal(passed[:, PAIR:].astype(F32))
+            ),
+        )
+        trans_last, base_last = out[:, :PAIR], out[:, PAIR:] + base_both
+
+        @pl.when(z > 0)
+        def _():
+            z_arrival(z - 1)
+
+            @pl.when(z > 1)
+            def _():
+                z_seen[2, 0] = z_slots[z - 1, 0]
+
+            z_seen[2, 1] = z_slots[z - 1, 1]
 
     with jax.named_scope("z_compose"):
-        p0, p1, p2 = (slot(z_seen, k) for k in range(3))
-        inner = dot1(p1[0], diagonal(p0[1])) + p1[1]
-        out = dot3(trans_both, beside(diagonal(p2[0]), diagonal(p2[1])))
-        states = dot3(out[:, :PAIR], diagonal(inner)) + (out[:, PAIR:] + base_both)
+        entering = through(plane_below(2), far)
+        states = dot3(trans_last, diagonal(entering)) + base_last
         state_first, state_second = states[:HEAD], states[HEAD:]
         mine = jnp.where(is_first, state_first, state_second)
         pair_states[0] = jnp.where(is_first, state_second, state_first)
@@ -496,7 +579,8 @@
 
     def read_pair(p, state, half):
         readout = local_rows[p] + dot3(carried_rows[p], diagonal(state))
-        mix_out = (group_norm(readout, ones, HEAD_EPS) * gate_gain[p]).astype(BF16)
+        scale = lax.rsqrt(dot2(readout * readout, ones) * (1.0 / HEAD) + HEAD_EPS)
+        mix_out = (readout * scale * gate_gain[p]).astype(BF16)
         started = []
         for k in range(4):
             mix_sent[half, k] = mix_out[k * 64 : (k + 1) * 64]
@@ -515,9 +599,17 @@
     with jax.named_scope("read_own"):
         started = read_pair(core, mine, 0)
 
-    with jax.named_scope("conv_project_out"):
-        loads[1].wait()
-        acc[...] = dot(conv_full[0, tp], conv_out_w[pl.ds(pl.multiple_of(tp * PAIR, PAIR), PAIR), :])
+    with jax.named_scope("own_out"):
+        loads[3].wait()
+        loads[4].wait()
+        acc[...] = dot(
+            conv_full[0, tp], conv_out_w[pl.ds(pl.multiple_of(tp * PAIR, PAIR), PAIR), :]
+        ) + dot(mix_sent[0, tp], mix_out_w[out_rows(tp, core), :])
+    with jax.named_scope("state_wait"):
+        state_copy.wait()
+    with jax.named_scope("read_other"):
+        started += read_pair(1 - core, pair_states[1], 1)
+    with jax.named_scope("conv_out"):
         for step in (1, 3, 2):
             arrived = x_of(4 - step)
             remote(
@@ -526,15 +618,23 @@
             ).wait_recv()
             rows = pl.ds(pl.multiple_of(arrived * PAIR, PAIR), PAIR)
             acc[...] += dot(conv_full[1, arrived], conv_out_w[rows, :])
-    with jax.named_scope("state_wait"):
-        state_copy.wait()
-    with jax.named_scope("read_other"):
-        started += read_pair(1 - core, pair_states[1], 1)
     with jax.named_scope("mix_own"):
-        loads[2].wait()
-        acc[...] += dot(mix_sent[0, tp], mix_out_w[out_rows(tp, core), :]) + dot(
-            mix_sent[1, tp], mix_out_w[out_rows(tp, 1 - core), :]
-        )
+        acc[...] += dot(mix_sent[1, tp], mix_out_w[out_rows(tp, 1 - core), :])
+    for copy in conv_copies:
+        copy.wait_send()
+    pl.when(sp < 31)(halo_copy.wait_send)
+    for step in (1, 2, 3):
+        pl.when(y_sends(step))(lambda step=step: y_copy(step, y, y_target(step)).wait_send())
+
+        @pl.when(z + step < 4)
+        def _(step=step):
+            z_copy(step, 1, z, sp + 8 * step).wait_send()
+            pl.when(z > 0)(z_copy(step, 0, z, sp + 8 * step).wait_send)
+
+        pl.when((y == 3) & (z + step < 4))(
+            lambda step=step: raw_copy(step, y, z, raw_target(step)).wait_send()
+        )
+
     for half in (0, 1):
         for step in (1, 3, 2):
             arrived = x_of(4 - step)
@@ -546,12 +646,10 @@
             with jax.named_scope("mix_project"):
                 p = core if half == 0 else 1 - core
                 acc[...] += dot(mix_full[half, arrived], mix_out_w[out_rows(arrived, p), :])
-    out_ref[...] = acc[...].astype(BF16)
-    for copy in y_copies + conv_copies + started:
+    with jax.named_scope("final"):
+        out_ref[...] = acc[...].astype(BF16)
+    for copy in started:
         copy.wait_send()
-    pl.when(sp < 31)(halo_copy.wait_send)
-    for step in (1, 2, 3):
-        pl.when(z + step < 4)(z_copy(step).wait_send)
 
 
 VMEM = pl.BlockSpec(memory_space=pltpu.VMEM)
@@ -592,7 +690,9 @@
             pltpu.VMEM((64, 256), F32),
             pltpu.VMEM((2, 64, 128), F32),
             pltpu.VMEM((4, 64, 256), BF16),
-            pltpu.VMEM((4, 64, 256), BF16),
+            pltpu.VMEM((4, 2, 64, 128), BF16),
+            pltpu.VMEM((3, 64, 256), BF16),
+            pltpu.VMEM((3, 2, 64, 128), BF16),
             pltpu.VMEM((3, 64, 256), BF16),
             pltpu.VMEM((3, 64, 256), BF16),
             pltpu.VMEM((288, 128), F32),
@@ -605,8 +705,8 @@
             pltpu.VMEM((2, 4, 64, 128), BF16),
             pltpu.VMEM((2, 4, 64, 128), BF16),
             pltpu.VMEM((64, 2048), F32),
-            dma((10,)), dma((3,)), dma((2,)), dma((2,)), dma((3,)), dma((3,)), dma((3,)), dma((3,)),
-            dma((1,)), dma((1,)), dma((3,)), dma((3,)), dma((2, 3)), dma((2, 3)), dma((7,)),
+            dma((8,)), dma((5,)), dma((2,)), dma((2,)), dma((3,)), dma((3,)), dma((3, 2)), dma((3, 2)),
+            dma((1,)), dma((1,)), dma((3,)), dma((3,)), dma((2, 3)), dma((2, 3)), dma((7,)), dma((3,)), dma((3,)),
         ],
         compiler_params=pltpu.CompilerParams(
             collective_id=0, has_side_effects=True, vmem_limit_bytes=56000000

time: 25.2 us -> 24.5 us (0.972)
  Pallas kernels: 24.4 us -> 23.7 us
    pallas_call x1, Pallas kernels: 24.4 us -> 23.7 us  [local(): pl.pallas_call(layer_kernel, name='layer', out_shape=pltpu.VMEM((64, 2048...]
where the time goes in v4:
time: 24.5 us; the launch traced here: 24.4 us
  Pallas kernels  23.7 us (97%)
  local copies, waits for them, and re-layouts  0.71 us (3%)
    pallas_call x1, Pallas kernels, local(): pl.pallas_call(layer_kernel, name='layer', out_shape=pltpu.VMEM((64, 2048...  23.7 us
    unnamed x1, local copies, waits for them, and re-layouts  0.71 us

profile of v4, /device:TPU:96, one launch (start us, length us, event | category | flops | bytes accessed | tf_op | source)
XLA Modules:
  0.0 24.4 jit_solution(9594490192756154985)
XLA Ops:
  0.0 23.7 %layer.1 = bf16[64,2048]{1,0:T(8,128)(2,1)S(1)} custom-call(bf16[256,2048]{1,0:T(8,128)(2,1)} %tokens_hbm.1, f32[1,2048]{1,0:T(1,128)} %bitcast.6, bf16[2048,256]{1,0:T(8,128)(2,1)} %decay_hbm.1, bf16[2048,256]{1,0:T(8,128)(2,1)} %key_hbm.1, bf16[2048,256]{1,0:T(8,128)(2,1)} %rate_hbm.1, bf16[2048,256]{1,0:T(8,128)(2,1)} %receptance_hbm.1, ...), custom_call_target="tpu_custom_call" | custom-call | tf_op jit(solution)/shard_map/layer/pallas_call | solution.py:667
  23.7 0.7 %copy.22 = bf16[64,2048]{1,0:T(8,128)(2,1)} copy(bf16[64,2048]{1,0:T(8,128)(2,1)S(1)} %layer.1) | data formatting | bytes 524288

commit v5 on v4

--- a/solution.py
+++ b/solution.py
@@ -219,8 +219,8 @@
     tokens, normed, weights, shift, extra, gate_w, conv_out_w, mix_out_w,
     totals, peer_total, pair_states, y_slots, z_slots, y_seen, z_seen, raw_slots, raw_seen, extended, halo, conv_rows,
     local_rows, carried_rows, gate_gain, conv_full, mix_sent, mix_full, acc,
-    sems, load_sems, pair_send, pair_recv, y_send, y_recv, z_send, z_recv, halo_send, halo_recv,
-    conv_send, conv_recv, mix_send, mix_recv, small_sems, raw_send, raw_recv,
+    sems, pair_send, pair_recv, y_send, y_recv, z_send, z_recv, halo_send, halo_recv,
+    conv_send, conv_recv, mix_send, mix_recv, raw_send, raw_recv,
 ):
     sp, tp = lax.axis_index("sp"), lax.axis_index("tp")
     core = lax.rem(sp, 2)
@@ -249,32 +249,24 @@
         )
 
     order = (decay_hbm, key_hbm, rate_hbm, receptance_hbm, value_hbm)
-    copies = [pltpu.make_async_copy(tokens_hbm, tokens, sems.at[0])]
+    def load(source, target, k):
+        return pltpu.make_async_copy(source, target, sems.at[k])
+
+    copies = [load(tokens_hbm, tokens, 0)]
     for i, source in enumerate(order):
-        copies.append(pltpu.make_async_copy(source, weights.at[i], sems.at[1 + i]))
-    late = [
-        pltpu.make_async_copy(shift_hbm, shift, sems.at[6]),
-        pltpu.make_async_copy(extra_hbm, extra, sems.at[7]),
-    ]
-    smalls = [
-        pltpu.make_async_copy(source, target, small_sems.at[i])
-        for i, (source, target) in enumerate(
-            (
-                (gain_hbm, gain_ref),
-                (key_gain_hbm, key_gain_ref),
-                (bias_hbm, bias_ref),
-                (taps_hbm, taps_ref),
-                (group_gain_hbm, group_gain_ref),
-                (group_shift_hbm, group_shift_ref),
-                (head_gain_hbm, head_gain_ref),
-            )
-        )
+        copies.append(load(source, weights.at[i], 1 + i))
+    late = [load(shift_hbm, shift, 6), load(extra_hbm, extra, 7)]
+    gain_copy = load(gain_hbm, gain_ref, 8)
+    smalls = [load(key_gain_hbm, key_gain_ref, 0), load(bias_hbm, bias_ref, 8)]
+    rest = [
+        load(taps_hbm, taps_ref, 1),
+        load(group_gain_hbm, group_gain_ref, 2),
+        load(group_shift_hbm, group_shift_ref, 3),
+        load(head_gain_hbm, head_gain_ref, 4),
     ]
     copies[0].start()
-    smalls[0].start()
+    gain_copy.start()
     for copy in copies[1:] + late:
-        copy.start()
-    for copy in smalls[1:]:
         copy.start()
 
     barrier = pltpu.get_barrier_semaphore()
@@ -298,13 +290,11 @@
     )
 
     loads = [
-        pltpu.make_async_copy(gate_hbm, gate_w, load_sems.at[0]),
-        pltpu.make_async_copy(conv_value_hbm, weights.at[5, :, pl.ds(0, PAIR)], load_sems.at[3]),
-        pltpu.make_async_copy(
-            conv_gate_hbm, weights.at[5, :, pl.ds(PAIR, PAIR)], load_sems.at[4]
-        ),
-        pltpu.make_async_copy(conv_out_hbm, conv_out_w, load_sems.at[1]),
-        pltpu.make_async_copy(mix_out_hbm, mix_out_w, load_sems.at[2]),
+        load(gate_hbm, gate_w, 0),
+        load(conv_value_hbm, weights.at[5, :, pl.ds(0, PAIR)], 8),
+        load(conv_gate_hbm, weights.at[5, :, pl.ds(PAIR, PAIR)], 5),
+        load(conv_out_hbm, conv_out_w, 6),
+        load(mix_out_hbm, mix_out_w, 7),
     ]
     eye = (iota((HEAD, 2 * PAIR), 0) == iota((HEAD, 2 * PAIR), 1) % HEAD) & (
         iota((HEAD, 2 * PAIR), 1) < PAIR
@@ -317,7 +307,9 @@
         z_seen[k, 1] = identity[:, PAIR:]
     with jax.named_scope("wait_tokens"):
         copies[0].wait()
-        smalls[0].wait()
+        gain_copy.wait()
+        for copy in smalls:
+            copy.start()
     with jax.named_scope("norm"):
         normed[...] = normalize(tokens[...], gain_ref[...])
     with jax.named_scope("project"):
@@ -335,10 +327,10 @@
             + keep * dot(normed[:, half:], weights[4, half:, :])
         )
         decay, key, rate, receptance, value = (rounded(rows) for rows in found)
-        for copy in late + smalls[1:]:
+        for copy in late + smalls:
             copy.wait()
-    for load in loads:
-        load.start()
+    for copy in loads[:3] + rest + loads[3:]:
+        copy.start()
     with jax.named_scope("algebra"):
         units = chunk_algebra(
             receptance, key, value, decay, rate, key_gain_ref[...], bias_ref[...], shift[...],
@@ -360,8 +352,8 @@
     pair_copy.start()
 
     with jax.named_scope("conv_project"):
-        for load in loads[:3]:
-            load.wait()
+        for copy in loads[:3]:
+            copy.wait()
         gate_rows = dot(normed[...], gate_w[...])
         conv_both = rounded(dot(normed[...], weights[5]))
         conv_input = (conv_both[:, :PAIR] * sigmoid(conv_both[:, PAIR:])).astype(BF16)
@@ -372,6 +364,8 @@
         extended[32:, :] = conv_input.astype(F32)
 
     with jax.named_scope("gate_project"):
+        for copy in rest:
+            copy.wait()
         gated = sigmoid(rounded(gate_rows)) * head_gain_ref[...]
         gate_gain[0] = gated[:, :PAIR]
         gate_gain[1] = gated[:, PAIR:]
@@ -467,24 +461,20 @@
         conv_out = (affine * sigmoid(affine)).astype(BF16)
         for k in range(4):
             conv_full[0, k] = conv_out[k * 64 : (k + 1) * 64]
-    conv_copies = []
     for step in (2, 1, 3):
         copy = remote(
             conv_full.at[0, x_of(step)], conv_full.at[1, tp],
-            conv_send.at[step - 1], conv_recv.at[step - 1], x_peer(step),
+            conv_send.at[0], conv_recv.at[0], x_peer(step),
         )
         copy.start()
-        conv_copies.append(copy)
-
-    def z_copy(up, kind, slot, peer):
-        return remote(
-            z_slots.at[slot, kind], z_slots.at[slot, kind], z_send.at[up - 1, kind],
-            z_recv.at[slot, kind], (peer, tp),
-        )
+
+    def z_copy(up, slot, peer, whole):
+        part = z_slots.at[slot] if whole else z_slots.at[slot, 1]
+        return remote(part, part, z_send.at[up - 1], z_recv.at[slot], (peer, tp))
 
     def z_column(up):
-        z_copy(up, 1, z, sp + 8 * up).start()
-        pl.when(z > 0)(z_copy(up, 0, z, sp + 8 * up).start)
+        pl.when(z > 0)(lambda: z_copy(up, z, sp + 8 * up, True).start())
+        pl.when(z == 0)(lambda: z_copy(up, z, sp + 8 * up, False).start())
 
     def upper(step):
         y_copy(step, lax.rem(y + 4 - step, 4), sibling).wait_recv()
@@ -514,11 +504,8 @@
             pl.when(z < 1)(lambda: z_column(3))
 
     def z_arrival(below):
-        @pl.when(below > 0)
-        def _():
-            z_copy(1, 0, below, sibling).wait_recv()
-
-        z_copy(1, 1, below, sibling).wait_recv()
+        pl.when(below > 0)(lambda: z_copy(1, below, sibling, True).wait_recv())
+        pl.when(below == 0)(lambda: z_copy(1, below, sibling, False).wait_recv())
 
     with jax.named_scope("z_wait"):
         for below in range(2):
@@ -571,7 +558,7 @@
         mine = jnp.where(is_first, state_first, state_second)
         pair_states[0] = jnp.where(is_first, state_second, state_first)
     state_copy = remote(
-        pair_states.at[0], pair_states.at[1], pair_send.at[1], pair_recv.at[1], (sibling, tp)
+        pair_states.at[0], pair_states.at[1], pair_send.at[0], pair_recv.at[1], (sibling, tp)
     )
     state_copy.start()
 
@@ -581,23 +568,20 @@
         readout = local_rows[p] + dot3(carried_rows[p], diagonal(state))
         scale = lax.rsqrt(dot2(readout * readout, ones) * (1.0 / HEAD) + HEAD_EPS)
         mix_out = (readout * scale * gate_gain[p]).astype(BF16)
-        started = []
         for k in range(4):
             mix_sent[half, k] = mix_out[k * 64 : (k + 1) * 64]
         for step in (2, 1, 3):
             copy = remote(
                 mix_sent.at[half, x_of(step)], mix_full.at[half, tp],
-                mix_send.at[half, step - 1], mix_recv.at[half, step - 1], x_peer(step),
+                mix_send.at[half], mix_recv.at[half, step - 1], x_peer(step),
             )
             copy.start()
-            started.append(copy)
-        return started
 
     def out_rows(owner, p):
         return pl.ds(pl.multiple_of(owner * 256 + p * PAIR, PAIR), PAIR)
 
     with jax.named_scope("read_own"):
-        started = read_pair(core, mine, 0)
+        read_pair(core, mine, 0)
 
     with jax.named_scope("own_out"):
         loads[3].wait()
@@ -608,28 +592,28 @@
     with jax.named_scope("state_wait"):
         state_copy.wait()
     with jax.named_scope("read_other"):
-        started += read_pair(1 - core, pair_states[1], 1)
+        read_pair(1 - core, pair_states[1], 1)
+    conv_all = remote(
+        conv_full.at[0, pl.ds(0, 3)], conv_full.at[1, pl.ds(0, 3)], conv_send.at[0],
+        conv_recv.at[0], x_peer(1),
+    )
     with jax.named_scope("conv_out"):
+        conv_all.wait_recv()
         for step in (1, 3, 2):
             arrived = x_of(4 - step)
-            remote(
-                conv_full.at[0, arrived], conv_full.at[1, arrived],
-                conv_send.at[step - 1], conv_recv.at[step - 1], x_peer(step),
-            ).wait_recv()
             rows = pl.ds(pl.multiple_of(arrived * PAIR, PAIR), PAIR)
             acc[...] += dot(conv_full[1, arrived], conv_out_w[rows, :])
     with jax.named_scope("mix_own"):
         acc[...] += dot(mix_sent[1, tp], mix_out_w[out_rows(tp, 1 - core), :])
-    for copy in conv_copies:
-        copy.wait_send()
+    conv_all.wait_send()
     pl.when(sp < 31)(halo_copy.wait_send)
     for step in (1, 2, 3):
         pl.when(y_sends(step))(lambda step=step: y_copy(step, y, y_target(step)).wait_send())
 
         @pl.when(z + step < 4)
         def _(step=step):
-            z_copy(step, 1, z, sp + 8 * step).wait_send()
-            pl.when(z > 0)(z_copy(step, 0, z, sp + 8 * step).wait_send)
+            pl.when(z > 0)(lambda: z_copy(step, z, sp + 8 * step, True).wait_send())
+            pl.when(z == 0)(lambda: z_copy(step, z, sp + 8 * step, False).wait_send())
 
         pl.when((y == 3) & (z + step < 4))(
             lambda step=step: raw_copy(step, y, z, raw_target(step)).wait_send()
@@ -641,15 +625,16 @@
             with jax.named_scope("mix_wait"):
                 remote(
                     mix_sent.at[half, arrived], mix_full.at[half, arrived],
-                    mix_send.at[half, step - 1], mix_recv.at[half, step - 1], x_peer(step),
+                    mix_send.at[half], mix_recv.at[half, step - 1], x_peer(step),
                 ).wait_recv()
             with jax.named_scope("mix_project"):
                 p = core if half == 0 else 1 - core
                 acc[...] += dot(mix_full[half, arrived], mix_out_w[out_rows(arrived, p), :])
     with jax.named_scope("final"):
         out_ref[...] = acc[...].astype(BF16)
-    for copy in started:
-        copy.wait_send()
+    for half in (0, 1):
+        block = mix_sent.at[half, pl.ds(0, 3)]
+        remote(block, block, mix_send.at[half], mix_recv.at[half, 0], x_peer(1)).wait_send()
 
 
 VMEM = pl.BlockSpec(memory_space=pltpu.VMEM)
@@ -705,8 +690,8 @@
             pltpu.VMEM((2, 4, 64, 128), BF16),
             pltpu.VMEM((2, 4, 64, 128), BF16),
             pltpu.VMEM((64, 2048), F32),
-            dma((8,)), dma((5,)), dma((2,)), dma((2,)), dma((3,)), dma((3,)), dma((3, 2)), dma((3, 2)),
-            dma((1,)), dma((1,)), dma((3,)), dma((3,)), dma((2, 3)), dma((2, 3)), dma((7,)), dma((3,)), dma((3,)),
+            dma((9,)), dma((1,)), dma((2,)), dma((3,)), dma((3,)), dma((3,)), dma((3,)),
+            dma((1,)), dma((1,)), dma((1,)), dma((1,)), dma((2,)), dma((2, 3)), dma((3,)), dma((3,)),
         ],
         compiler_params=pltpu.CompilerParams(
             collective_id=0, has_side_effects=True, vmem_limit_bytes=56000000

time: 24.5 us -> 24.3 us (level)
    pallas_call x1, Pallas kernels: 23.7 us -> 23.5 us  [local(): pl.pallas_call(layer_kernel, name='layer', out_shape=pltpu.VMEM((64, 2048...]
where the time goes in v5:
time: 24.3 us; the launch traced here: 24.2 us
  Pallas kernels  23.5 us (97%)
  local copies, waits for them, and re-layouts  0.71 us (3%)
    pallas_call x1, Pallas kernels, local(): pl.pallas_call(layer_kernel, name='layer', out_shape=pltpu.VMEM((64, 2048...  23.5 us
    unnamed x1, local copies, waits for them, and re-layouts  0.71 us

profile of v5, /device:TPU:96, one launch (start us, length us, event | category | flops | bytes accessed | tf_op | source)
XLA Modules:
  0.0 24.2 jit_solution(3323299323900014176)
XLA Ops:
  0.0 23.5 %layer.1 = bf16[64,2048]{1,0:T(8,128)(2,1)S(1)} custom-call(bf16[256,2048]{1,0:T(8,128)(2,1)} %tokens_hbm.1, f32[1,2048]{1,0:T(1,128)} %bitcast.6, bf16[2048,256]{1,0:T(8,128)(2,1)} %decay_hbm.1, bf16[2048,256]{1,0:T(8,128)(2,1)} %key_hbm.1, bf16[2048,256]{1,0:T(8,128)(2,1)} %rate_hbm.1, bf16[2048,256]{1,0:T(8,128)(2,1)} %receptance_hbm.1, ...), custom_call_target="tpu_custom_call" | custom-call | tf_op jit(solution)/shard_map/layer/pallas_call | solution.py:652
  23.5 0.7 %copy.22 = bf16[64,2048]{1,0:T(8,128)(2,1)} copy(bf16[64,2048]{1,0:T(8,128)(2,1)S(1)} %layer.1) | data formatting | bytes 524288

commit v6 on v5

--- a/solution.py
+++ b/solution.py
@@ -252,7 +252,9 @@
     def load(source, target, k):
         return pltpu.make_async_copy(source, target, sems.at[k])
 
-    copies = [load(tokens_hbm, tokens, 0)]
+    upper_rows, lower_rows = pl.ds(0, 128), pl.ds(128, 128)
+    copies = [load(tokens_hbm.at[upper_rows], tokens.at[upper_rows], 0)]
+    second_copy = load(tokens_hbm.at[lower_rows], tokens.at[lower_rows], 9)
     for i, source in enumerate(order):
         copies.append(load(source, weights.at[i], 1 + i))
     late = [load(shift_hbm, shift, 6), load(extra_hbm, extra, 7)]
@@ -265,8 +267,12 @@
         load(head_gain_hbm, head_gain_ref, 4),
     ]
     copies[0].start()
+    second_copy.start()
     gain_copy.start()
-    for copy in copies[1:] + late:
+    for i, source in enumerate(order):
+        for rows in (pl.ds(0, 1024), pl.ds(1024, 1024)):
+            load(source.at[rows], weights.at[i, rows], 1 + i).start()
+    for copy in late:
         copy.start()
 
     barrier = pltpu.get_barrier_semaphore()
@@ -311,7 +317,9 @@
         for copy in smalls:
             copy.start()
     with jax.named_scope("norm"):
-        normed[...] = normalize(tokens[...], gain_ref[...])
+        normed[:128, :] = normalize(tokens[:128, :], gain_ref[...])
+        second_copy.wait()
+        normed[128:, :] = normalize(tokens[128:, :], gain_ref[...])
     with jax.named_scope("project"):
         found = []
         for i in (0, 2):
@@ -444,6 +452,41 @@
         trans_both = jnp.concatenate([before_chip[0], before_second[0]], axis=0)
         base_both = jnp.concatenate([before_chip[1], before_second[1]], axis=0)
 
+    def z_copy(up, slot, peer, whole):
+        part = z_slots.at[slot] if whole else z_slots.at[slot, 1]
+        return remote(part, part, z_send.at[up - 1], z_recv.at[slot], (peer, tp))
+
+    def z_column(up):
+        pl.when(z > 0)(lambda: z_copy(up, z, sp + 8 * up, True).start())
+        pl.when(z == 0)(lambda: z_copy(up, z, sp + 8 * up, False).start())
+
+    def upper(step):
+        y_copy(step, lax.rem(y + 4 - step, 4), sibling).wait_recv()
+
+    with jax.named_scope("plane"):
+
+        @pl.when(z < 3)
+        def _():
+            pl.when(y < 3)(lambda: upper(3))
+            lower = compose(slot(y_slots, 1), slot(y_slots, 0), dot1)
+            pl.when(y < 2)(lambda: upper(2))
+
+            def store(total):
+                z_slots[z, 0] = total[0].astype(BF16)
+                z_slots[z, 1] = total[1].astype(BF16)
+
+            @pl.when(y == 0)
+            def _():
+                store(compose(slot(y_slots, 2), lower, dot3))
+
+            @pl.when(y > 0)
+            def _():
+                store(compose(compose(slot(y_slots, 3), slot(y_slots, 2), dot1), lower, dot3))
+
+            z_column(1)
+            pl.when(z < 2)(lambda: z_column(2))
+            pl.when(z < 1)(lambda: z_column(3))
+
     with jax.named_scope("halo_wait"):
 
         @pl.when(sp > 0)
@@ -467,41 +510,6 @@
             conv_send.at[0], conv_recv.at[0], x_peer(step),
         )
         copy.start()
-
-    def z_copy(up, slot, peer, whole):
-        part = z_slots.at[slot] if whole else z_slots.at[slot, 1]
-        return remote(part, part, z_send.at[up - 1], z_recv.at[slot], (peer, tp))
-
-    def z_column(up):
-        pl.when(z > 0)(lambda: z_copy(up, z, sp + 8 * up, True).start())
-        pl.when(z == 0)(lambda: z_copy(up, z, sp + 8 * up, False).start())
-
-    def upper(step):
-        y_copy(step, lax.rem(y + 4 - step, 4), sibling).wait_recv()
-
-    with jax.named_scope("plane"):
-
-        @pl.when(z < 3)
-        def _():
-            for step in (3, 2):
-                pl.when(step > y)(lambda step=step: upper(step))
-            lower = compose(slot(y_slots, 1), slot(y_slots, 0), dot1)
-
-            def store(total):
-                z_slots[z, 0] = total[0].astype(BF16)
-                z_slots[z, 1] = total[1].astype(BF16)
-
-            @pl.when(y == 0)
-            def _():
-                store(compose(slot(y_slots, 2), lower, dot3))
-
-            @pl.when(y > 0)
-            def _():
-                store(compose(compose(slot(y_slots, 3), slot(y_slots, 2), dot1), lower, dot3))
-
-            z_column(1)
-            pl.when(z < 2)(lambda: z_column(2))
-            pl.when(z < 1)(lambda: z_column(3))
 
     def z_arrival(below):
         pl.when(below > 0)(lambda: z_copy(1, below, sibling, True).wait_recv())
@@ -690,7 +698,7 @@
             pltpu.VMEM((2, 4, 64, 128), BF16),
             pltpu.VMEM((2, 4, 64, 128), BF16),
             pltpu.VMEM((64, 2048), F32),
-            dma((9,)), dma((1,)), dma((2,)), dma((3,)), dma((3,)), dma((3,)), dma((3,)),
+            dma((10,)), dma((1,)), dma((2,)), dma((3,)), dma((3,)), dma((3,)), dma((3,)),
             dma((1,)), dma((1,)), dma((1,)), dma((1,)), dma((2,)), dma((2, 3)), dma((3,)), dma((3,)),
         ],
         compiler_params=pltpu.CompilerParams(

time: 24.3 us -> 24.1 us (level)
  no operation moved by 1% of the time
where the time goes in v6:
time: 24.1 us; the launch traced here: 24 us
  Pallas kernels  23.3 us (97%)
  local copies, waits for them, and re-layouts  0.71 us (3%)
    pallas_call x1, Pallas kernels, local(): pl.pallas_call(layer_kernel, name='layer', out_shape=pltpu.VMEM((64, 2048...  23.3 us
    unnamed x1, local copies, waits for them, and re-layouts  0.71 us

profile of v6, /device:TPU:96, one launch (start us, length us, event | category | flops | bytes accessed | tf_op | source)
XLA Modules:
  0.0 24.0 jit_solution(965300787755076352)
XLA Ops:
  0.0 23.3 %layer.1 = bf16[64,2048]{1,0:T(8,128)(2,1)S(1)} custom-call(bf16[256,2048]{1,0:T(8,128)(2,1)} %tokens_hbm.1, f32[1,2048]{1,0:T(1,128)} %bitcast.6, bf16[2048,256]{1,0:T(8,128)(2,1)} %decay_hbm.1, bf16[2048,256]{1,0:T(8,128)(2,1)} %key_hbm.1, bf16[2048,256]{1,0:T(8,128)(2,1)} %rate_hbm.1, bf16[2048,256]{1,0:T(8,128)(2,1)} %receptance_hbm.1, ...), custom_call_target="tpu_custom_call" | custom-call | tf_op jit(solution)/shard_map/layer/pallas_call | solution.py:660
  23.3 0.7 %copy.22 = bf16[64,2048]{1,0:T(8,128)(2,1)} copy(bf16[64,2048]{1,0:T(8,128)(2,1)S(1)} %layer.1) | data formatting | bytes 524288
